TPU v7x, 32 devices: a whole 2x2x4 slice. The times are simulated.
32 devices in a mesh: sp: 8 (over z, y), tp: 4 (over x, core).
Axes of the slice: x: 2, y: 2, z: 4, core: 2. Of those that a mesh axis runs over, the one named last changes fastest.
Arguments:
- stream: bfloat16 [1024, 2048], P('sp'), may hold values from -12 to 12
- out_grad: bfloat16 [1024, 2048], P('sp'), may hold values from -6 to 6
- routes: int32 [1024, 2], P('sp'), may hold values from 0 to 7, all different within a row; in each aligned block of 128 rows (0 to 127, 128 to 255, ...) at most 64 rows name the same one
- route_weight: float32 [1024, 2], P('sp'), may hold values from 0.2 to 1
- queries: bfloat16 [1024, 8, 128], P('sp', 'tp'), may hold values from -6 to 6
- key_vectors: bfloat16 [1024, 8, 128], P('sp', 'tp'), may hold values from -6 to 6
- value_vectors: bfloat16 [1024, 8, 256], P('sp', 'tp'), may hold values from -6 to 6
- log_decay: float32 [1024, 8], P('sp', 'tp'), may hold values from -1 to 0
- out_proj: bfloat16 [2048, 2048], P(None, 'tp'), may hold values from -0.125 to 0.125
- gate_weight: bfloat16 [8, 2048, 1024], P('sp', None, 'tp'), may hold values from -0.125 to 0.125
- up_weight: bfloat16 [8, 2048, 1024], P('sp', None, 'tp'), may hold values from -0.125 to 0.125
- down_weight: bfloat16 [8, 1024, 2048], P('sp', 'tp'), may hold values from -0.1875 to 0.1875
Outputs:
- gate_grad: bfloat16 [8, 2048, 1024], P('sp', None, 'tp')
- up_grad: bfloat16 [8, 2048, 1024], P('sp', None, 'tp')
- down_grad: bfloat16 [8, 1024, 2048], P('sp', 'tp')
- proj_grad: float32 [2048, 2048], P('sp', 'tp')
- query_grad: bfloat16 [1024, 8, 128], P('sp', 'tp')
- key_grad: bfloat16 [1024, 8, 128], P('sp', 'tp')
- value_grad: bfloat16 [1024, 8, 256], P('sp', 'tp')
Inputs may be any that keep to these rules, and one draw needn't show every extreme that they name: `routes`: each row names two different experts. In each aligned block of 128 rows no expert is named by more than 64 rows, and in some block an expert is named by exactly 64.
All inputs are finite; a program needn't handle non-finite values.
Results may differ from a plain program's by a relative error of at most 0.025.
Values may be sent and summed in bfloat16 or wider, within the bound.
A program may use at most 128 MiB of HBM per device.

v0:
```python
import jax
import jax.numpy as jnp
from jax import lax
from jax.sharding import PartitionSpec as P

CLAMP_LIMIT = 7.0
GATE_SLOPE = 1.702
EPSILON = 1e-06
TOP_PRECISION = lax.Precision.HIGHEST


def prefix(x, axis, join, neutral):
    place = lax.axis_index(axis)
    gathered = jax.tree.map(
        lambda a, kind: lax.all_gather(a.astype(kind), axis), x, (jnp.bfloat16, jnp.bfloat16)
    )
    state = jax.tree.map(lambda a, e: jnp.zeros_like(a) + jnp.asarray(e, a.dtype), x, neutral)

    def one(hop, state):
        return join(
            state,
            jax.tree.map(
                lambda a, own: lax.dynamic_index_in_dim(a, hop, 0, False).astype(own.dtype),
                gathered,
                x,
            ),
        )

    return lax.fori_loop(0, place, one, state)


def prefix_2(x, axis, join, neutral):
    count = lax.axis_size(axis)
    place = lax.axis_index(axis)
    ahead = count - 1 - place
    gathered = jax.tree.map(
        lambda a, kind: lax.all_gather(a.astype(kind), axis),
        x,
        jax.tree.map(lambda a: jnp.bfloat16 if a.dtype == jnp.float32 else a.dtype, x),
    )
    state = jax.tree.map(lambda a, e: jnp.zeros_like(a) + jnp.asarray(e, a.dtype), x, neutral)

    def one(hop, state):
        source = count - 1 - hop
        return join(
            state,
            jax.tree.map(
                lambda a, own: lax.dynamic_index_in_dim(a, source, 0, False).astype(own.dtype),
                gathered,
                x,
            ),
        )

    return lax.fori_loop(0, ahead, one, state)


def slot_numbers(route_block, expert_count):
    flat_ids = route_block.reshape(-1)
    onehot = (flat_ids[:, None] == jnp.arange(expert_count, dtype=jnp.int32)[None, :]).astype(
        jnp.int32
    )
    before = jnp.cumsum(onehot, axis=0) - onehot
    return (flat_ids, jnp.sum(before * onehot, axis=1))


def rotation_tables(start, count, key_width):
    frequency = 1.0 / 10000.0 ** jnp.linspace(0.0, 1.0, key_width // 2, dtype=jnp.float32)
    token_position = (start + jnp.arange(count, dtype=jnp.int32)).astype(jnp.float32)
    angles = token_position[:, None] * frequency[None, :]
    return (jnp.cos(angles), jnp.sin(angles))


def turn(field, cosines, sines):
    paired = field.reshape(field.shape[:-1] + (field.shape[-1] // 2, 2))
    even_part = paired[..., 0]
    odd_part = paired[..., 1]
    cos_rows = cosines[:, None, :]
    sin_rows = sines[:, None, :]
    turned = jnp.stack(
        [even_part * cos_rows - odd_part * sin_rows, odd_part * cos_rows + even_part * sin_rows],
        axis=-1,
    )
    return turned.reshape(field.shape)


def decay_combine(earlier, next_rows):
    return (earlier[0] * next_rows[0], next_rows[1] + next_rows[0][:, None, None] * earlier[1])


def expert_local(routed_rows, routed_grads, gate_w, up_w, down_w):
    gate_pre = jnp.dot(routed_rows, gate_w, preferred_element_type=jnp.float32)
    up_pre = jnp.dot(routed_rows, up_w, preferred_element_type=jnp.float32)
    gate_clip = jnp.minimum(gate_pre, CLAMP_LIMIT)
    up_clip = jnp.clip(up_pre, -CLAMP_LIMIT, CLAMP_LIMIT)
    sigmoid_gate = jax.nn.sigmoid(GATE_SLOPE * gate_clip)
    activated = (gate_clip * sigmoid_gate * (up_clip + 1.0)).astype(jnp.bfloat16)
    down_part = lax.dot_general(
        activated, routed_grads, (((0,), (0,)), ((), ())), preferred_element_type=jnp.float32
    )
    act_grad = lax.dot_general(
        routed_grads, down_w, (((1,), (1,)), ((), ())), preferred_element_type=jnp.float32
    )
    slope = sigmoid_gate + GATE_SLOPE * gate_clip * sigmoid_gate * (1.0 - sigmoid_gate)
    gate_pre_grad = jnp.where(
        gate_pre < CLAMP_LIMIT, act_grad * (up_clip + 1.0) * slope, 0.0
    ).astype(jnp.bfloat16)
    up_pre_grad = jnp.where(
        jnp.abs(up_pre) < CLAMP_LIMIT, act_grad * gate_clip * sigmoid_gate, 0.0
    ).astype(jnp.bfloat16)
    gate_part = lax.dot_general(
        routed_rows, gate_pre_grad, (((0,), (0,)), ((), ())), preferred_element_type=jnp.float32
    )
    up_part = lax.dot_general(
        routed_rows, up_pre_grad, (((0,), (0,)), ((), ())), preferred_element_type=jnp.float32
    )
    back_rows = lax.dot_general(
        gate_pre_grad, gate_w, (((1,), (1,)), ((), ())), preferred_element_type=jnp.float32
    )
    back_rows = back_rows + lax.dot_general(
        up_pre_grad, up_w, (((1,), (1,)), ((), ())), preferred_element_type=jnp.float32
    )
    return (
        gate_part.astype(jnp.bfloat16),
        up_part.astype(jnp.bfloat16),
        down_part.astype(jnp.bfloat16),
        back_rows.astype(jnp.bfloat16),
    )


def per_device(
    stream,
    out_grad,
    routes,
    route_weight,
    queries,
    key_vectors,
    value_vectors,
    log_decay,
    out_proj,
    gate_weight,
    up_weight,
    down_weight,
):
    experts = lax.axis_size("sp")
    tokens_here = stream.shape[0]
    model_width = stream.shape[1]
    capacity = 4 * tokens_here // experts
    pair_count = 2 * tokens_here
    flat_ids, slot_ids = slot_numbers(routes, experts)
    destination = flat_ids * capacity + slot_ids
    source = (
        jnp.full((experts * capacity,), -1, jnp.int32)
        .at[destination]
        .set(jnp.arange(pair_count, dtype=jnp.int32))
    )
    present = (source >= 0)[:, None]
    picked = jnp.maximum(source, 0)
    zero_value = jnp.zeros((), jnp.bfloat16)
    pair_grad = (route_weight[:, :, None] * out_grad[:, None, :].astype(jnp.float32)).astype(
        jnp.bfloat16
    )
    pair_grad = pair_grad.reshape(pair_count, model_width)
    send_rows = jnp.where(present, jnp.take(stream, picked // 2, axis=0), zero_value)
    send_rows = send_rows.reshape(experts, capacity, model_width)
    send_grads = jnp.where(present, jnp.take(pair_grad, picked, axis=0), zero_value)
    send_grads = send_grads.reshape(experts, capacity, model_width)
    quarter = model_width // lax.axis_size("tp")
    col_start = lax.axis_index("tp") * quarter
    quarters = (
        lax.dynamic_slice_in_dim(send_rows, col_start, quarter, 2),
        lax.dynamic_slice_in_dim(send_grads, col_start, quarter, 2),
    )
    quarters = (
        lax.all_to_all(quarters[0], "sp", split_axis=0, concat_axis=0, tiled=True),
        lax.all_to_all(quarters[1], "sp", split_axis=0, concat_axis=0, tiled=True),
    )
    routed_rows, routed_grads = (
        lax.all_gather(quarters[0], "tp", axis=2, tiled=True),
        lax.all_gather(quarters[1], "tp", axis=2, tiled=True),
    )
    routed_rows = routed_rows.reshape(experts * capacity, model_width)
    routed_grads = routed_grads.reshape(experts * capacity, model_width)
    gate_part, up_part, down_part, back_rows = expert_local(
        routed_rows, routed_grads, gate_weight[0], up_weight[0], down_weight[0]
    )
    summed = lax.psum(back_rows, "tp").astype(jnp.float32).astype(jnp.bfloat16)
    returned = lax.all_to_all(
        summed.reshape(experts, capacity, model_width),
        "sp",
        split_axis=0,
        concat_axis=0,
        tiled=True,
    )
    returned = returned.reshape(experts * capacity, model_width)
    per_pair = (
        jnp.take(returned, destination, axis=0)
        .reshape(tokens_here, 2, model_width)
        .astype(jnp.float32)
    )
    resid_grad = (out_grad.astype(jnp.float32) + per_pair[:, 0] + per_pair[:, 1]).astype(
        jnp.bfloat16
    )
    heads_local = queries.shape[1]
    key_width = queries.shape[2]
    value_width = value_vectors.shape[2]
    key_scale = key_width ** (-0.5)
    cosines, sines = rotation_tables(lax.axis_index("sp") * tokens_here, tokens_here, key_width)
    query_rotated = turn(queries.astype(jnp.float32), cosines, sines).transpose(1, 0, 2)
    key_rotated = (turn(key_vectors.astype(jnp.float32), cosines, sines) * key_scale).transpose(
        1, 0, 2
    )
    value_per_head = value_vectors.astype(jnp.float32).transpose(1, 0, 2)
    running_total = jnp.cumsum(log_decay, axis=0).T
    block_total = running_total[:, -1]
    causal = (jnp.arange(tokens_here)[:, None] >= jnp.arange(tokens_here)[None, :])[None]
    difference = running_total[:, :, None] - running_total[:, None, :]
    decay_mask = jnp.where(causal, jnp.exp(jnp.where(causal, difference, 0.0)), 0.0)
    per_head_decay = jnp.exp(running_total)
    remaining_decay = jnp.exp(block_total[:, None] - running_total)
    carried = jnp.exp(block_total)
    inner_state = jnp.einsum(
        "wfs,wfi->wsi",
        key_rotated * remaining_decay[..., None],
        value_per_head,
        precision=TOP_PRECISION,
    )
    identity = (jnp.ones_like(carried), jnp.zeros_like(inner_state))
    incoming_state = prefix((carried, inner_state), "sp", decay_combine, identity)[1]
    weights = (
        jnp.einsum("hik,hjk->hij", query_rotated, key_rotated, precision=TOP_PRECISION) * decay_mask
    )
    retained_output = jnp.einsum("hij,hjv->hiv", weights, value_per_head, precision=TOP_PRECISION)
    retained_output = retained_output + per_head_decay[..., None] * jnp.einsum(
        "dzr,drs->dzs", query_rotated, incoming_state, precision=TOP_PRECISION
    )
    inverse_rms = lax.rsqrt(
        jnp.mean(retained_output * retained_output, axis=-1, keepdims=True) + EPSILON
    )
    normed = retained_output * inverse_rms
    normed_bf = (
        normed.transpose(1, 0, 2)
        .reshape(tokens_here, heads_local * value_width)
        .astype(jnp.bfloat16)
    )
    proj_grad = lax.psum_scatter(
        lax.dot_general(
            resid_grad, normed_bf, (((0,), (0,)), ((), ())), preferred_element_type=jnp.float32
        ),
        "sp",
        scatter_dimension=0,
        tiled=True,
    )
    normed_grad = jnp.dot(resid_grad, out_proj, preferred_element_type=jnp.float32)
    normed_grad = normed_grad.reshape(tokens_here, heads_local, value_width).transpose(1, 0, 2)
    retention_gradient = inverse_rms * (
        normed_grad - normed * jnp.mean(normed_grad * normed, axis=-1, keepdims=True)
    )
    inner_gradient = jnp.einsum(
        "gwn,gwj->gnj",
        query_rotated * per_head_decay[..., None],
        retention_gradient,
        precision=TOP_PRECISION,
    )
    future_gradient = prefix_2((carried, inner_gradient), "sp", decay_combine, identity)[1]
    score_grad = (
        jnp.einsum("hiv,hjv->hij", retention_gradient, value_per_head, precision=TOP_PRECISION)
        * decay_mask
    )
    query_portion = jnp.einsum("hij,hjk->hik", score_grad, key_rotated, precision=TOP_PRECISION)
    query_portion = query_portion + per_head_decay[..., None] * jnp.einsum(
        "bpl,btl->bpt", retention_gradient, incoming_state, precision=TOP_PRECISION
    )
    key_portion = jnp.einsum("hij,hik->hjk", score_grad, query_rotated, precision=TOP_PRECISION)
    key_portion = key_portion + remaining_decay[..., None] * jnp.einsum(
        "uxn,ubn->uxb", value_per_head, future_gradient, precision=TOP_PRECISION
    )
    value_portion = jnp.einsum("hij,hiv->hjv", weights, retention_gradient, precision=TOP_PRECISION)
    value_portion = value_portion + remaining_decay[..., None] * jnp.einsum(
        "bui,bim->bum", key_rotated, future_gradient, precision=TOP_PRECISION
    )
    query_grad = turn(query_portion.transpose(1, 0, 2), cosines, -sines).astype(jnp.bfloat16)
    key_grad = (turn(key_portion.transpose(1, 0, 2), cosines, -sines) * key_scale).astype(
        jnp.bfloat16
    )
    value_grad = value_portion.transpose(1, 0, 2).astype(jnp.bfloat16)
    return (
        gate_part[None],
        up_part[None],
        down_part[None],
        proj_grad,
        query_grad,
        key_grad,
        value_grad,
    )


def solution(mesh):
    in_specs = (
        P("sp", None),
        P("sp", None),
        P("sp", None),
        P("sp", None),
        P("sp", "tp", None),
        P("sp", "tp", None),
        P("sp", "tp", None),
        P("sp", "tp"),
        P(None, "tp"),
        P("sp", None, "tp"),
        P("sp", None, "tp"),
        P("sp", "tp", None),
    )
    out_specs = (
        P("sp", None, "tp"),
        P("sp", None, "tp"),
        P("sp", "tp", None),
        P("sp", "tp"),
        P("sp", "tp", None),
        P("sp", "tp", None),
        P("sp", "tp", None),
    )
    return jax.shard_map(
        per_device, mesh=mesh, in_specs=in_specs, out_specs=out_specs, check_vma=False
    )
```

profile of v0, /device:TPU:0, one launch (start us, length us, event | category | flops | bytes accessed | tf_op | source)
XLA Modules:
  0.0 386.7 jit_solution(6628498509636234050)
XLA Ops:
  8.1 0.8 broadcast_multiply_fusion.1
  8.9 0.8 copy.152
  11.2 1.4 scatter_custom_fusion
  12.6 3.5 mul.382
  16.1 3.7 mul.383
  20.3 2.7 multiply_convert_fusion
  23.0 6.6 %gather_fusion.1 = bf16[512,2048]{1,0:T(8,128)(2,1)} fusion(bf16[256,2048]{1,0:T(8,128)(2,1)} %multiply_convert_fusion, s32[1024]{0:T(1024)S(1)} %pad_clamp_fusion.1), kind=kCustom, calls=%fused_computation.1 | custom fusion | bytes 4196352 | tf_op jit(solution)/shard_map/jit(_take)/gather | solution.py:165
  29.7 3.3 gather_fusion
  33.0 1.5 fusion.23
  34.6 21.9 %all_to_all.15 = bf16[8,64,512]{2,1,0:T(8,128)(2,1)} all-to-all(bf16[8,64,512]{2,1,0:T(8,128)(2,1)S(1)} %get-tuple-element.222), channel_id=1, replica_groups=mesh['sp'=8,'tp'=4] {'sp'}, dimensions={0} | all-to-all | bytes 1048576 | tf_op jit(solution)/shard_map/all_to_all | solution.py:174
  56.5 17.6 %all_to_all.16 = bf16[8,64,512]{2,1,0:T(8,128)(2,1)} all-to-all(bf16[8,64,512]{2,1,0:T(8,128)(2,1)S(1)} %get-tuple-element.221), channel_id=1, replica_groups=mesh['sp'=8,'tp'=4] {'sp'}, dimensions={0} | all-to-all | bytes 1048576 | tf_op jit(solution)/shard_map/all_to_all | solution.py:175
  74.7 3.5 all-gather.8.cloned.1.call-done
  78.2 3.5 fusion.14
  81.7 1.5 fusion.20
  83.2 19.1 %all-gather.10.cloned.1.call-done = bf16[8,64,2048]{2,1,0:T(8,128)(2,1)} async-done(((bf16[8,64,512]{2,1,0:T(8,128)(2,1)}), bf16[8,64,2048]{2,1,0:T(8,128)(2,1)}) %all-gather.10.cloned.1.call-update) | async-done | bytes 2097168 | tf_op jit(solution)/shard_map/all_gather | solution.py:179
  102.3 3.1 select_convert_fusion
  105.5 0.7 fusion.18
  106.3 0.6 copy-done.15
  106.9 2.1 add_convert_fusion
  109.2 0.8 fusion.47
  111.4 1.0 convolution_convert_fusion.4
  112.5 48.1 %all-reduce.3.cloned.1.call-done = bf16[8,64,2048]{2,1,0:T(8,128)(2,1)} async-done(((bf16[8,64,2048]{2,1,0:T(8,128)(2,1)}), bf16[8,64,2048]{2,1,0:T(8,128)(2,1)}) %all-reduce.3.cloned.1.call-update) | async-done | bytes 2097168 | tf_op jit(solution)/shard_map/psum | solution.py:186
  160.6 5.5 %all-to-all-start.2 = ((bf16[8,64,2048]{2,1,0:T(8,128)(2,1)}), bf16[8,64,2048]{2,1,0:T(8,128)(2,1)}, u32[]{:S(2)}, u32[]{:S(2)}) async-start(bf16[8,64,2048]{2,1,0:T(8,128)(2,1)} %all-reduce.3.cloned.1.call-done), calls=%async_computation.2 | async-start | bytes 4194304 | tf_op jit(solution)/shard_map/all_to_all | solution.py:187
  167.9 48.0 %all-reduce = bf16[16]{0:T(256)(128)(2,1)S(1)} all-reduce(bf16[16]{0:T(256)(128)(2,1)S(1)} %dynamic-update-slice), channel_id=3, replica_groups=mesh['sp'=8,'tp'=4] {'sp'}, use_global_device_ids=true, to_apply=%add | all-reduce | flops 16 | bytes 64
  216.2 0.6 pad_clamp_fusion
  219.1 1.1 multiply_reduce_fusion
  220.1 0.6 add_rsqrt_fusion
  220.7 4.4 %gather_fusion.2 = bf16[256,2048]{1,0:T(8,128)(2,1)S(1)} fusion(bf16[512,2048]{1,0:T(8,128)(2,1)} %bitcast.19, s32[1024]{0:T(1024)} %pad_clamp_fusion), kind=kCustom, calls=%fused_computation.2 | custom fusion | bytes 2098176 | tf_op jit(solution)/shard_map/jit(_take)/gather | solution.py:196
  225.1 1.5 gather.23
  226.6 2.0 fusion.22
  228.8 1.6 fusion.62
  230.4 1.1 copy.169
  231.5 0.9 fusion.25
  232.4 1.1 fusion.26
  233.5 2.1 convolution_convert_fusion.3
  235.8 1.5 subtract_exponential_fusion
  237.4 0.6 copy-done.30
  238.0 1.2 fusion.29
  239.3 2.7 fusion.61
  242.0 0.8 copy-done.19
  242.8 0.6 copy.174
  243.5 3.5 fusion
  247.0 1.7 fusion.1
  249.2 1.8 fusion.2
  252.8 35.5 %all-gather.14.cloned.1.call-done = bf16[16,128,256]{2,1,0:T(8,128)(2,1)} async-done(((bf16[2,128,256]{2,1,0:T(8,128)(2,1)}), bf16[16,128,256]{2,1,0:T(8,128)(2,1)}) %all-gather.14.cloned.1.call-update) | async-done | bytes 1048592 | tf_op jit(solution)/shard_map/all_gather | solution.py:37
  288.4 12.1 %while.27 = (s32[]{:T(128)}, f32[2,128,256]{2,1,0:T(8,128)S(1)}, s32[]{:T(128)}, bf16[8,2,128,256]{3,2,1,0:T(8,128)(2,1)}, bf16[8,2]{1,0:T(8,128)(2,1)}, /*index=5*/s32[]{:T(128)}, s32[]{:T(128)}, s32[]{:T(128)}, s32[]{:T(128)}) while((s32[]{:T(128)}, f32[2,128,256]{2,1,0:T(8,128)S(1)}, s32[]{:T(128)}, bf16[8,2,128,256]{3,2,1,0:T(8,128)(2,1)}, ...), condition=%wide.region_12.13_spmd, body=%wide.region_11.12_spmd.sunk | while | flops 196616 | bytes 655535 | solution.py:54
  288.4 0.7 bitcast_convert_fusion.5
  289.1 1.0 convert_add_fusion.5
  290.1 0.7 bitcast_convert_fusion.5
  290.8 1.0 convert_add_fusion.5
  291.9 0.7 bitcast_convert_fusion.5
  292.6 1.0 convert_add_fusion.5
  293.6 0.7 bitcast_convert_fusion.5
  294.3 1.0 convert_add_fusion.5
  295.3 0.7 bitcast_convert_fusion.5
  296.0 1.0 convert_add_fusion.5
  297.0 0.7 bitcast_convert_fusion.5
  297.7 1.1 convert_add_fusion.5
  298.8 0.7 bitcast_convert_fusion.5
  299.5 1.0 convert_add_fusion.5
  301.3 0.8 copy.179
  302.2 0.8 copy.180
  303.4 0.8 copy.181
  304.2 75.2 %reduce-scatter.2.cloned.1.call-done = f32[256,512]{1,0:T(8,128)} async-done(((f32[2048,512]{1,0:T(8,128)}), f32[256,512]{1,0:T(8,128)}) %reduce-scatter.2.cloned.1.call-update) | async-done | bytes 524304 | tf_op jit(solution)/shard_map/reduce_scatter | solution.py:245
  (164 shorter events, 12.0 us)
Async XLA Ops:
  8.0 220.8 %copy-start = (bf16[2048,512]{1,0:T(8,128)(2,1)S(1)}, bf16[2048,512]{1,0:T(8,128)(2,1)}, u32[]{:S(2)}) copy-start(bf16[2048,512]{1,0:T(8,128)(2,1)} %param.24) | copy-start | bytes 6291460
  8.0 70.2 %all-gather.8.cloned.1.call-start = ((), (), s32[]{:S(2)}) async-start(), calls=%async_computation.4 | async-start | bytes 2621440 | tf_op jit(solution)/shard_map/all_gather | solution.py:178
  16.1 3.7 copy-start.36
  23.0 6.7 %copy-start.1 = (bf16[128,2048]{1,0:T(8,128)(2,1)S(1)}, bf16[128,2048]{1,0:T(8,128)(2,1)}, u32[]{:S(2)}) copy-start(bf16[128,2048]{1,0:T(8,128)(2,1)} %param.16) | copy-start | bytes 1572868
  34.5 39.7 %copy-start.25 = (bf16[128,2,128]{2,1,0:T(2,128)(2,1)S(1)}, bf16[128,2,128]{2,1,0:T(2,128)(2,1)}, u32[]{:S(2)}) copy-start(bf16[128,2,128]{2,1,0:T(2,128)(2,1)} %param.20) | copy-start | bytes 196612
  34.6 39.9 %copy-start.26 = (bf16[128,2,128]{2,1,0:T(2,128)(2,1)S(1)}, bf16[128,2,128]{2,1,0:T(2,128)(2,1)}, u32[]{:S(2)}) copy-start(bf16[128,2,128]{2,1,0:T(2,128)(2,1)} %param.21) | copy-start | bytes 196612
  56.5 45.9 %all-gather.10.cloned.1.call-start = ((), (), s32[]{:S(2)}) async-start(), calls=%async_computation.5 | async-start | bytes 2621440 | tf_op jit(solution)/shard_map/all_gather | solution.py:179
  74.2 86.4 %all-reduce.3.cloned.1.call-start = ((), (), s32[]{:S(2)}) async-start(), calls=%async_computation.6 | async-start | bytes 4194304 | tf_op jit(solution)/shard_map/psum | solution.py:186
  74.4 7.3 %copy-start.14 = (bf16[1,2048,256]{2,1,0:T(8,128)(2,1)S(1)}, bf16[1,2048,256]{2,1,0:T(8,128)(2,1)}, u32[]{:S(2)}) copy-start(bf16[1,2048,256]{2,1,0:T(8,128)(2,1)} %param.25) | copy-start | bytes 3145732
  78.2 3.5 copy-start.38
  105.5 0.8 copy-start.20
  105.5 0.8 copy-start.22
  105.5 1.4 copy-start.15
  109.0 1.8 copy-start.37
  109.0 2.4 copy-start.6
  109.0 108.9 %all-gather.12.cloned.1.call-start = ((), (), s32[]{:S(2)}) async-start(), calls=%async_computation.8 | async-start | bytes 1179648 | tf_op jit(solution)/shard_map/all_gather | solution.py:15
  110.0 50.5 %copy-start.17 = (f32[128,64]{0,1:T(8,128)}, f32[128,64]{0,1:T(8,128)S(1)}, u32[]{:S(2)}) copy-start(f32[128,64]{0,1:T(8,128)S(1)} %get-tuple-element.216) | copy-start | bytes 98308
  110.6 50.0 %copy-start.8 = (f32[128,2,64,2]{0,3,2,1:T(2,128)}, f32[128,2,64,2]{0,3,2,1:T(2,128)S(1)}, u32[]{:S(2)}) copy-start(f32[128,2,64,2]{0,3,2,1:T(2,128)S(1)} %get-tuple-element.225) | copy-start | bytes 393220
  110.6 105.5 %copy-start.10 = (f32[128,2,64,2]{0,3,2,1:T(2,128)}, f32[128,2,64,2]{0,3,2,1:T(2,128)S(1)}, u32[]{:S(2)}) copy-start(f32[128,2,64,2]{0,3,2,1:T(2,128)S(1)} %get-tuple-element.224) | copy-start | bytes 393220
  111.0 49.5 %copy-start.16 = (f32[128,2]{1,0:T(8,128)}, f32[128,2]{1,0:T(8,128)S(1)}, u32[]{:S(2)}) copy-start(f32[128,2]{1,0:T(8,128)S(1)} %reduce_window_sum.28) | copy-start | bytes 3076
  111.1 106.4 %copy-start.27 = (f32[128,2]{0,1:T(2,128)}, f32[128,2]{0,1:T(2,128)S(1)}, u32[]{:S(2)}) copy-start(f32[128,2]{0,1:T(2,128)S(1)} %copy.162) | copy-start | bytes 3076
  111.3 49.3 %copy-start.34 = (f32[2]{0:T(128)}, f32[2]{0:T(128)S(1)}, u32[]{:S(2)}) copy-start(f32[2]{0:T(128)S(1)} %slice_reduce_fusion.1) | copy-start | bytes 28
  111.4 107.0 %copy-start.33 = (f32[2,128]{1,0:T(2,128)}, f32[2,128]{1,0:T(2,128)S(1)}, u32[]{:S(2)}) copy-start(f32[2,128]{1,0:T(2,128)S(1)} %get-tuple-element.219) | copy-start | bytes 3076
  112.4 53.7 %copy-start.41 = (u32[32]{0:T(128)S(1)}, u32[32]{0:T(128)}, u32[]{:S(2)}) copy-start(u32[32]{0:T(128)} %constant.181) | copy-start | bytes 388
  112.5 104.4 %copy-start.32 = (s32[128,2]{0,1:T(2,128)S(1)}, s32[128,2]{0,1:T(2,128)}, u32[]{:S(2)}) copy-start(s32[128,2]{0,1:T(2,128)} %param.18) | copy-start | bytes 3076
  160.6 60.1 %all-to-all-start.2 = ((bf16[8,64,2048]{2,1,0:T(8,128)(2,1)}), bf16[8,64,2048]{2,1,0:T(8,128)(2,1)}, u32[]{:S(2)}, u32[]{:S(2)}) async-start(bf16[8,64,2048]{2,1,0:T(8,128)(2,1)} %all-reduce.3.cloned.1.call-done), calls=%async_computation.2 | async-start | bytes 4194304 | tf_op jit(solution)/shard_map/all_to_all | solution.py:187
  166.1 122.2 %all-gather.14.cloned.1.call-start = ((), (), s32[]{:S(2)}) async-start(), calls=%async_computation.9 | async-start | bytes 1179648 | tf_op jit(solution)/shard_map/all_gather | solution.py:37
  216.2 2.1 copy-start.4
  217.9 0.6 copy-start.12
  218.0 2.7 copy-start.35
  218.4 0.7 copy-start.3
  226.6 2.0 copy-start.5
  228.8 2.7 copy-start.2
  235.6 143.8 %reduce-scatter.2.cloned.1.call-start = ((), (), s32[]{:S(2)}) async-start(), calls=%async_computation.7 | async-start | bytes 4718592 | tf_op jit(solution)/shard_map/reduce_scatter | solution.py:245
  237.4 0.6 copy-start.30
  242.0 0.8 copy-start.19
  242.0 1.5 copy-start.21
  243.5 3.5 copy-start.23
  243.5 3.5 copy-start.39
  247.0 1.8 copy-start.40
  247.0 1.8 copy-start.42
  247.0 2.2 copy-start.43
  249.2 1.8 copy-start.7
  249.2 1.8 copy-start.28
  249.2 2.1 copy-start.11
  249.2 2.4 copy-start.9
  249.2 2.8 copy-start.13
  249.2 3.2 copy-start.31
  252.4 48.1 %copy-start.29 = (f32[128,2]{0,1:T(2,128)S(1)}, f32[128,2]{0,1:T(2,128)}, u32[]{:S(2)}) copy-start(f32[128,2]{0,1:T(2,128)} %copy.174) | copy-start | bytes 3076
  288.4 12.5 %copy-start.18 = (f32[128,64]{0,1:T(8,128)S(1)}, f32[128,64]{0,1:T(8,128)}, u32[]{:S(2)}) copy-start(f32[128,64]{0,1:T(8,128)} %copy-done.17) | copy-start | bytes 98308
  288.4 12.5 %copy-start.24 = (f32[128,64]{0,1:T(8,128)S(1)}, f32[128,64]{0,1:T(8,128)}, u32[]{:S(2)}) copy-start(f32[128,64]{0,1:T(8,128)} %get-tuple-element.214) | copy-start | bytes 98308
Sparse Core Ops, SparseCore 0:
  56.6 21.5 all-gather.7
  79.7 22.5 all-gather.9
  109.1 51.4 all-reduce.2
Sparse Core Ops, SparseCore 1:
  112.5 40.3 all-gather.11
  235.6 52.7 all-gather.13
  292.4 86.9 reduce-scatter.1
where the time goes:
time: 388 us; the launch traced here: 387 us
  waiting for transfers between devices  182 us (47%)
  blocking collectives  87.5 us (23%)
  local copies, waits for them, and re-layouts  35.9 us (9%)
  matrix products  29.6 us (8%)
  other arithmetic  29 us (7%)
  between operations  16.8 us (4%)
  starting transfers between devices  6.18 us (2%)
    reduce_scatter x1, waiting for transfers between devices, per_device(): lax.psum_scatter(lax.dot_general(resid_grad, normed_bf, (((0,), (0,)), ((...  75.2 us
    psum x1, waiting for transfers between devices, per_device(): summed = lax.psum(back_rows, 'tp').astype(jnp.float32).astype(jnp.bfloat16)  48.1 us
    unnamed x1, blocking collectives  48 us
    all_gather x1, waiting for transfers between devices, prefix_2(): lax.all_gather(a.astype(kind), axis)  35.5 us
    all_to_all x1, blocking collectives, per_device(): lax.all_to_all(quarters[0], 'sp', split_axis=0, concat_axis=0, tiled=True)  21.9 us
    all_gather x1, waiting for transfers between devices, per_device(): lax.all_gather(quarters[1], 'tp', axis=2, tiled=True)  19.1 us
    all_to_all x1, blocking collectives, per_device(): lax.all_to_all(quarters[1], 'sp', split_axis=0, concat_axis=0, tiled=True)  17.6 us
  transfers between devices with their start and end apart: 7, of which 5 were waited for; matrix products, arithmetic and copies ran while one was open for 11% of the time, Pallas kernels for 0%

commit v1 on v0

v1 whole, which is shorter than its diff:
```python
import functools

import jax
import jax.numpy as jnp
from jax import lax
from jax.experimental import pallas as pl
from jax.experimental.pallas import tpu as pltpu
from jax.sharding import PartitionSpec as P

CLAMP_LIMIT = 7.0
GATE_SLOPE = 1.702
EPSILON = 1e-06
F32 = jnp.float32
BF16 = jnp.bfloat16
MESH = pl.DeviceIdType.MESH


def any_specs(count):
    return [pl.BlockSpec(memory_space=pl.ANY)] * count


def vmem_specs(count):
    return [pl.BlockSpec(memory_space=pltpu.VMEM)] * count


def tp_partners(c, n_tp):
    far = lax.rem(c + n_tp // 2, n_tp)
    near = c + 1 - 2 * lax.rem(c, 2)
    return far, near


def greet(n_sp, me, c, sp_peers, tp_peers):
    barrier = pltpu.get_barrier_semaphore()
    count = 0
    if sp_peers:
        for k in range(1, n_sp):
            pl.semaphore_signal(
                barrier, inc=1, device_id=(lax.rem(me + k, n_sp), c), device_id_type=MESH
            )
            count += 1
    for t in tp_peers:
        pl.semaphore_signal(barrier, inc=1, device_id=(me, t), device_id_type=MESH)
        count += 1
    pl.semaphore_wait(barrier, count)


def push(src, dst, send_sem, recv_sem, device):
    return pltpu.make_async_remote_copy(
        src_ref=src,
        dst_ref=dst,
        send_sem=send_sem,
        recv_sem=recv_sem,
        device_id=device,
        device_id_type=MESH,
    )


def dispatch_kernel(
    n_sp, n_tp, q, rows, grads, tot, rows_out, grads_out, tot_out,
    own_sem, ssem, rsem, xssem, xrsem, dssem, drsem, essem, ersem, tssem, trsem,
):
    me = lax.axis_index("sp")
    c = lax.axis_index("tp")
    far, near = tp_partners(c, n_tp)
    greet(n_sp, me, c, True, (far, near))
    arrays = ((rows, rows_out), (grads, grads_out))

    def cols(quarter):
        return pl.ds(pl.multiple_of(quarter * q, 128), q)

    waits = []
    for k in range(1, n_sp):
        peer = lax.rem(me + k, n_sp)
        cp = push(tot, tot_out.at[me], tssem.at[k], trsem.at[k], (peer, c))
        cp.start()
        waits.append(cp)
        for a, (src, out) in enumerate(arrays):
            cp = push(
                src.at[peer], out.at[me, :, cols(c)], ssem.at[a, k], rsem.at[a, k], (peer, c)
            )
            cp.start()
            waits.append(cp)
    local = [pltpu.make_async_copy(tot, tot_out.at[me], own_sem.at[2])]
    for a, (src, out) in enumerate(arrays):
        local.append(pltpu.make_async_copy(src.at[me], out.at[me, :, cols(c)], own_sem.at[a]))
    for cp in local:
        cp.start()
    sent = []
    last = []

    def relay(k):
        source = lax.rem(me + n_sp - k, n_sp)
        for a, (src, out) in enumerate(arrays):
            spot = out.at[source, :, cols(far)]
            push(spot, spot, xssem.at[a, k], xrsem.at[a, k], (me, far)).wait_recv()
            cp = push(spot, spot, essem.at[a, k], ersem.at[a, k], (me, near))
            cp.start()
            sent.append(cp)
            last.append((out, source, a, k))

    for k in range(n_sp):
        source = lax.rem(me + n_sp - k, n_sp)
        for a, (src, out) in enumerate(arrays):
            spot = out.at[source, :, cols(c)]
            if k == 0:
                origin = src.at[me]
            else:
                push(spot, spot, ssem.at[a, k], rsem.at[a, k], (me, far)).wait_recv()
                origin = spot
            for sems, device in (((xssem, xrsem), far), ((dssem, drsem), near)):
                cp = push(origin, spot, sems[0].at[a, k], sems[1].at[a, k], (me, device))
                cp.start()
                sent.append(cp)
        if k >= 1:
            relay(k - 1)
    relay(n_sp - 1)
    near_far = lax.rem(near + n_tp // 2, n_tp)
    for out, source, a, k in last:
        spot = out.at[source, :, cols(near)]
        push(spot, spot, dssem.at[a, k], drsem.at[a, k], (me, near)).wait_recv()
        spot = out.at[source, :, cols(near_far)]
        push(spot, spot, essem.at[a, k], ersem.at[a, k], (me, near)).wait_recv()
    for k in range(1, n_sp):
        source = lax.rem(me + n_sp - k, n_sp)
        spot = tot_out.at[source]
        push(spot, spot, tssem.at[k], trsem.at[k], (me, far)).wait_recv()
    for cp in waits + sent:
        cp.wait_send()
    for cp in local:
        cp.wait()


def dispatch(rows, grads, tot, n_tp):
    n_sp, cap, q = rows.shape
    full = jax.ShapeDtypeStruct((n_sp, cap, q * n_tp), rows.dtype)
    dma = pltpu.SemaphoreType.DMA
    return pl.pallas_call(
        functools.partial(dispatch_kernel, n_sp, n_tp, q),
        out_shape=(full, full, jax.ShapeDtypeStruct((n_sp,) + tot.shape, tot.dtype)),
        in_specs=any_specs(3),
        out_specs=tuple(any_specs(3)),
        scratch_shapes=[dma((3,))] + [dma((2, n_sp))] * 8 + [dma((n_sp,))] * 2,
        compiler_params=pltpu.CompilerParams(collective_id=0, has_side_effects=True),
        name="dispatch",
    )(rows, grads, tot)


def return_kernel(
    n_sp, n_tp, q, back, comb, og, resid,
    part, xbuf, xrecv, sendbuf, ret, resq,
    pssem, prsem, xssem, xrsem, ssem, rsem, gssem, grsem,
):
    me = lax.axis_index("sp")
    c = lax.axis_index("tp")
    far, near = tp_partners(c, n_tp)
    near_far = lax.rem(near + n_tp // 2, n_tp)
    greet(n_sp, me, c, True, (far, near))

    def cols(quarter):
        return pl.ds(pl.multiple_of(quarter * q, 128), q)

    order = list(range(1, n_sp)) + [0]
    waits = []
    for k in order:
        i = lax.rem(me + k, n_sp)
        for b, quarter in enumerate((near_far, near)):
            cp = push(
                back.at[i, :, cols(quarter)], part.at[b, k], pssem.at[b, k], prsem.at[b, k],
                (me, near),
            )
            cp.start()
            waits.append(cp)

    def to_far(k):
        cp = push(xbuf.at[k], xrecv.at[k], xssem.at[k], xrsem.at[k], (me, far))
        cp.start()
        waits.append(cp)

    def to_home(k):
        cp = push(
            sendbuf.at[k], ret.at[me], ssem.at[k], rsem.at[k], (lax.rem(me + k, n_sp), c)
        )
        cp.start()
        waits.append(cp)

    def first(k):
        i = lax.rem(me + k, n_sp)
        push(xbuf.at[k], part.at[0, k], pssem.at[0, k], prsem.at[0, k], (me, near)).wait_recv()
        xbuf[k] = (back[i, :, cols(far)].astype(F32) + part[0, k].astype(F32)).astype(BF16)

    def second(k):
        i = lax.rem(me + k, n_sp)
        push(xbuf.at[k], part.at[1, k], pssem.at[1, k], prsem.at[1, k], (me, near)).wait_recv()
        push(xbuf.at[k], xrecv.at[k], xssem.at[k], xrsem.at[k], (me, far)).wait_recv()
        total = (
            back[i, :, cols(c)].astype(F32) + part[1, k].astype(F32) + xrecv[k].astype(F32)
        ).astype(BF16)
        if k == 0:
            ret[me] = total
        else:
            sendbuf[k] = total

    lag = 2
    for n in range(n_sp + lag + 1):
        if n < n_sp:
            first(order[n])
        if 1 <= n <= n_sp:
            to_far(order[n - 1])
        if lag <= n < n_sp + lag:
            second(order[n - lag])
        if n >= lag + 1 and order[n - lag - 1] != 0:
            to_home(order[n - lag - 1])
    for k in range(1, n_sp):
        source = lax.rem(me + n_sp - k, n_sp)
        push(sendbuf.at[k], ret.at[source], ssem.at[k], rsem.at[k], (me, far)).wait_recv()
    cap = back.shape[1]
    returned = ret[...].astype(F32).reshape(n_sp * cap, q).astype(BF16)
    resq[...] = (
        og[...].astype(F32) + jnp.dot(comb[...], returned, preferred_element_type=F32)
    ).astype(BF16)
    mine = resid.at[:, cols(c)]
    own = pltpu.make_async_copy(resq, mine, gssem.at[3])
    own.start()
    for s, device in enumerate((far, near)):
        cp = push(resq, mine, gssem.at[s], grsem.at[s], (me, device))
        cp.start()
        waits.append(cp)
    spot = resid.at[:, cols(far)]
    push(resq, spot, gssem.at[0], grsem.at[0], (me, far)).wait_recv()
    cp = push(spot, spot, gssem.at[2], grsem.at[2], (me, near))
    cp.start()
    waits.append(cp)
    push(resq, resid.at[:, cols(near)], gssem.at[1], grsem.at[1], (me, near)).wait_recv()
    push(resq, resid.at[:, cols(near_far)], gssem.at[2], grsem.at[2], (me, near)).wait_recv()
    own.wait()
    for cp in waits:
        cp.wait_send()


def give_back(back, comb, og_q, n_tp):
    n_sp, cap, width = back.shape
    q = width // n_tp
    tokens = og_q.shape[0]
    dma = pltpu.SemaphoreType.DMA
    block = pltpu.VMEM((n_sp, cap, q), BF16)
    return pl.pallas_call(
        functools.partial(return_kernel, n_sp, n_tp, q),
        out_shape=jax.ShapeDtypeStruct((tokens, width), BF16),
        in_specs=vmem_specs(3),
        out_specs=pl.BlockSpec(memory_space=pl.ANY),
        scratch_shapes=[pltpu.VMEM((2, n_sp, cap, q), BF16)]
        + [block] * 4
        + [pltpu.VMEM((tokens, q), BF16)]
        + [dma((2, n_sp))] * 2
        + [dma((n_sp,))] * 4
        + [dma((4,)), dma((3,))],
        compiler_params=pltpu.CompilerParams(collective_id=1, has_side_effects=True),
        name="give_back",
    )(back, comb, og_q)


def swap_kernel(n_sp, w, resid, state, cols_out, states, own_sem, ssem, rsem):
    me = lax.axis_index("sp")
    c = lax.axis_index("tp")
    greet(n_sp, me, c, True, ())

    def part(index):
        if len(resid.shape) == 3:
            return resid.at[index]
        return resid.at[:, pl.ds(pl.multiple_of(index * w, 128), w)]

    waits = []
    for k in range(1, n_sp):
        peer = lax.rem(me + k, n_sp)
        for a, (src, out) in enumerate(((state, states), (part(peer), cols_out))):
            cp = push(src, out.at[me], ssem.at[a, k], rsem.at[a, k], (peer, c))
            cp.start()
            waits.append(cp)
    local = [
        pltpu.make_async_copy(part(me), cols_out.at[me], own_sem.at[0]),
        pltpu.make_async_copy(state, states.at[me], own_sem.at[1]),
    ]
    for cp in local:
        cp.start()
    for k in range(1, n_sp):
        source = lax.rem(me + n_sp - k, n_sp)
        for a, out in enumerate((states, cols_out)):
            spot = out.at[source]
            push(spot, spot, ssem.at[a, k], rsem.at[a, k], (source, c)).wait_recv()
    for cp in waits:
        cp.wait_send()
    for cp in local:
        cp.wait()


def swap(resid, state, n_sp):
    tokens, width = resid.shape
    w = width // n_sp
    if w % 128:
        resid = resid.reshape(tokens, n_sp, w).transpose(1, 0, 2)
    dma = pltpu.SemaphoreType.DMA
    return pl.pallas_call(
        functools.partial(swap_kernel, n_sp, w),
        out_shape=(
            jax.ShapeDtypeStruct((n_sp, tokens, w), BF16),
            jax.ShapeDtypeStruct((n_sp,) + state.shape, BF16),
        ),
        in_specs=any_specs(2),
        out_specs=tuple(any_specs(2)),
        scratch_shapes=[dma((2,)), dma((2, n_sp)), dma((2, n_sp))],
        compiler_params=pltpu.CompilerParams(collective_id=2, has_side_effects=True),
        name="swap",
    )(resid, state)


def rotation_tables(start, count, key_width):
    frequency = 1.0 / 10000.0 ** jnp.linspace(0.0, 1.0, key_width // 2, dtype=F32)
    frequency = jnp.repeat(frequency, 2)
    token_position = (start + jnp.arange(count, dtype=jnp.int32)).astype(F32)
    angles = token_position[:, None] * frequency[None, :]
    return (jnp.cos(angles)[None], jnp.sin(angles)[None])


def swap_matrix(key_width):
    row = jnp.arange(key_width)[:, None]
    col = jnp.arange(key_width)[None, :]
    up = (col == row + 1) & (row % 2 == 0)
    down = (col == row - 1) & (row % 2 == 1)
    return (up.astype(F32) - down.astype(F32)).astype(BF16)


def turn(field, cosines, sines, matrix):
    turned = jnp.einsum("htk,kl->htl", field.astype(BF16), matrix, preferred_element_type=F32)
    return field.astype(F32) * cosines + turned * sines


def ein(spec, a, b):
    return jnp.einsum(spec, a.astype(BF16), b.astype(BF16), preferred_element_type=F32)


def fine(spec, a, b):
    return jnp.einsum(spec, a.astype(F32), b.astype(F32), precision=lax.Precision.HIGHEST)


def mm(a, b, da, db):
    return lax.dot_general(a, b, (((da,), (db,)), ((), ())), preferred_element_type=F32)


def expert_local(routed_rows, routed_grads, gate_w, up_w, down_w):
    gate_pre = mm(routed_rows, gate_w, 1, 0)
    up_pre = mm(routed_rows, up_w, 1, 0)
    gate_clip = jnp.minimum(gate_pre, CLAMP_LIMIT)
    up_clip = jnp.clip(up_pre, -CLAMP_LIMIT, CLAMP_LIMIT)
    sigmoid_gate = jax.nn.sigmoid(GATE_SLOPE * gate_clip)
    activated = (gate_clip * sigmoid_gate * (up_clip + 1.0)).astype(BF16)
    down_part = mm(activated, routed_grads, 0, 0)
    act_grad = mm(routed_grads, down_w, 1, 1)
    slope = sigmoid_gate + GATE_SLOPE * gate_clip * sigmoid_gate * (1.0 - sigmoid_gate)
    gate_pre_grad = jnp.where(
        gate_pre < CLAMP_LIMIT, act_grad * (up_clip + 1.0) * slope, 0.0
    ).astype(BF16)
    up_pre_grad = jnp.where(
        jnp.abs(up_pre) < CLAMP_LIMIT, act_grad * gate_clip * sigmoid_gate, 0.0
    ).astype(BF16)
    gate_part = mm(routed_rows, gate_pre_grad, 0, 0)
    up_part = mm(routed_rows, up_pre_grad, 0, 0)
    back_rows = mm(gate_pre_grad, gate_w, 1, 1) + mm(up_pre_grad, up_w, 1, 1)
    return (
        gate_part.astype(BF16),
        up_part.astype(BF16),
        down_part.astype(BF16),
        back_rows.astype(BF16),
    )


def per_device(
    stream, out_grad, routes, route_weight, queries, key_vectors, value_vectors, log_decay,
    out_proj, gate_weight, up_weight, down_weight,
):
    n_sp = lax.axis_size("sp")
    n_tp = lax.axis_size("tp")
    me = lax.axis_index("sp")
    tokens, width = stream.shape
    capacity = 4 * tokens // n_sp
    slots = n_sp * capacity
    quarter = width // n_tp
    heads = queries.shape[1]
    key_width = queries.shape[2]
    value_width = value_vectors.shape[2]

    ids = jnp.arange(n_sp, dtype=jnp.int32)
    chosen = routes[:, :, None] == ids[None, None, :]
    counts = jnp.sum(chosen.astype(F32), axis=1).astype(BF16)
    place = jnp.arange(tokens)
    lower = (place[:, None] > place[None, :]).astype(BF16)
    before = jnp.dot(lower, counts, preferred_element_type=F32)
    slot = jnp.sum(jnp.where(chosen, before[:, None, :], 0.0), axis=2).astype(jnp.int32)
    target = routes * capacity + slot
    spots = jnp.arange(slots, dtype=jnp.int32)
    hit = target.T[:, None, :] == spots[None, :, None]
    pick = (hit[0] | hit[1]).astype(BF16)
    weight = jnp.sum(
        jnp.where(hit[0], route_weight[None, :, 0], 0.0)
        + jnp.where(hit[1], route_weight[None, :, 1], 0.0),
        axis=1,
    )
    comb = ((target[:, :1] == spots[None, :]) | (target[:, 1:] == spots[None, :])).astype(BF16)
    col_start = lax.axis_index("tp") * quarter
    stream_q = lax.dynamic_slice_in_dim(stream, col_start, quarter, 1)
    og_q = lax.dynamic_slice_in_dim(out_grad, col_start, quarter, 1)
    send_rows = jnp.dot(pick, stream_q, preferred_element_type=F32).astype(BF16)
    send_grads = (
        weight[:, None] * jnp.dot(pick, og_q, preferred_element_type=F32)
    ).astype(BF16)

    running = jnp.cumsum(log_decay, axis=0).T
    block_total = running[:, -1]
    tot = jnp.broadcast_to(jnp.pad(block_total, (0, 128 - heads))[None, :], (8, 128))
    rows, grads, tots = dispatch(
        send_rows.reshape(n_sp, capacity, quarter),
        send_grads.reshape(n_sp, capacity, quarter),
        tot,
        n_tp,
    )

    matrix = swap_matrix(key_width)
    cosines, sines = rotation_tables(me * tokens, tokens, key_width)
    scale = key_width ** (-0.5)
    query_rot = turn(queries.transpose(1, 0, 2), cosines, sines, matrix)
    key_rot = turn(key_vectors.transpose(1, 0, 2), cosines, sines, matrix) * scale
    values = value_vectors.transpose(1, 0, 2)
    causal = (place[:, None] >= place[None, :])[None]
    difference = running[:, :, None] - running[:, None, :]
    mask = jnp.where(causal, jnp.exp(jnp.where(causal, difference, 0.0)), 0.0)
    decay = jnp.exp(running)[..., None]
    remaining = jnp.exp(block_total[:, None] - running)[..., None]
    inner = ein("wfs,wfi->wsi", key_rot * remaining, values).astype(BF16)
    inner_all = lax.all_gather(inner, "sp")
    key_bf = key_rot.astype(BF16)
    query_bf = query_rot.astype(BF16)
    weights = fine("hik,hjk->hij", query_rot, key_rot) * mask
    retained_local = fine("hij,hjv->hiv", weights, values)

    gate_part, up_part, down_part, back_rows = expert_local(
        rows.reshape(slots, width),
        grads.reshape(slots, width),
        gate_weight[0],
        up_weight[0],
        down_weight[0],
    )
    totals = tots[:, 0, :heads]
    sums = jnp.cumsum(totals, axis=0)
    sum_before = jnp.sum(jnp.where((ids < me)[:, None], totals, 0.0), axis=0)
    sum_through = sum_before + block_total
    past = jnp.where((ids < me)[:, None], sum_before[None] - sums, 0.0)
    past = jnp.where((ids < me)[:, None], jnp.exp(past), 0.0)
    coming = jnp.where((ids > me)[:, None], sums - totals - sum_through[None], 0.0)
    coming = jnp.where((ids > me)[:, None], jnp.exp(coming), 0.0)
    incoming = jnp.sum(inner_all.astype(F32) * past[:, :, None, None], axis=0)
    retained = retained_local + decay * fine("dzr,drs->dzs", query_rot, incoming)
    inverse_rms = lax.rsqrt(jnp.mean(retained * retained, axis=-1, keepdims=True) + EPSILON)
    normed = retained * inverse_rms
    normed_bf = normed.transpose(1, 0, 2).reshape(tokens, heads * value_width).astype(BF16)
    normed_all = lax.all_gather(normed_bf, "sp", axis=0, tiled=True)

    resid = give_back(back_rows.reshape(n_sp, capacity, width), comb, og_q, n_tp)
    normed_grad = jnp.dot(resid, out_proj, preferred_element_type=F32)
    normed_grad = normed_grad.reshape(tokens, heads, value_width).transpose(1, 0, 2)
    grad = inverse_rms * (
        normed_grad - normed * jnp.mean(normed_grad * normed, axis=-1, keepdims=True)
    )
    grad_bf = grad.astype(BF16)
    inner_grad = ein("gwn,gwj->gnj", query_rot * decay, grad_bf).astype(BF16)
    resid_cols, grads_all = swap(resid, inner_grad, n_sp)
    future = jnp.sum(grads_all.astype(F32) * coming[:, :, None, None], axis=0).astype(BF16)
    score = fine("hiv,hjv->hij", grad, values) * mask
    query_portion = ein("hij,hjk->hik", score, key_bf) + decay * fine(
        "bpl,btl->bpt", grad, incoming
    )
    key_portion = ein("hij,hik->hjk", score, query_bf) + remaining * ein(
        "uxn,ubn->uxb", values, future
    )
    value_portion = ein("hij,hiv->hjv", weights, grad_bf) + remaining * ein(
        "bui,bim->bum", key_bf, future
    )
    query_grad = turn(query_portion, cosines, -sines, matrix).astype(BF16).transpose(1, 0, 2)
    key_grad = (
        (turn(key_portion, cosines, -sines, matrix) * scale).astype(BF16).transpose(1, 0, 2)
    )
    value_grad = value_portion.astype(BF16).transpose(1, 0, 2)
    proj_grad = mm(resid_cols.reshape(n_sp * tokens, -1), normed_all, 0, 0)
    return (
        gate_part[None],
        up_part[None],
        down_part[None],
        proj_grad,
        query_grad,
        key_grad,
        value_grad,
    )


def solution(mesh):
    in_specs = (
        P("sp", None),
        P("sp", None),
        P("sp", None),
        P("sp", None),
        P("sp", "tp", None),
        P("sp", "tp", None),
        P("sp", "tp", None),
        P("sp", "tp"),
        P(None, "tp"),
        P("sp", None, "tp"),
        P("sp", None, "tp"),
        P("sp", "tp", None),
    )
    out_specs = (
        P("sp", None, "tp"),
        P("sp", None, "tp"),
        P("sp", "tp", None),
        P("sp", "tp"),
        P("sp", "tp", None),
        P("sp", "tp", None),
        P("sp", "tp", None),
    )
    return jax.shard_map(
        per_device, mesh=mesh, in_specs=in_specs, out_specs=out_specs, check_vma=False
    )
```

time: 388 us -> 233 us (0.60)
  waiting for transfers between devices: 182 us -> 39.7 us
  Pallas kernels: 0 us -> 112 us
  blocking collectives: 87.5 us -> 0 us
  other arithmetic: 29 us -> 11.7 us
  local copies, waits for them, and re-layouts: 35.9 us -> 18.7 us
  matrix products: 29.6 us -> 36 us
  starting transfers between devices: 6.18 us -> 0.08 us
    pallas_call x0 -> x3, Pallas kernels: none -> 112 us  [the longest x1 42.3 us: dispatch(): pl.pallas_call(functools.partial(dispatch_kernel, n_sp, n_tp, q), out_sha...]
    reduce_scatter x1 -> x0, waiting for transfers between devices: 75.2 us -> none  [per_device(): lax.psum_scatter(lax.dot_general(resid_grad, normed_bf, (((0,), (0,)), ((...]
    psum x1 -> x0, waiting for transfers between devices: 48.1 us -> none  [per_device(): summed = lax.psum(back_rows, 'tp').astype(jnp.float32).astype(jnp.bfloat16)]
    unnamed x1 -> x0, blocking collectives: 48 us -> none
    all_to_all x2 -> x0, blocking collectives: 39.5 us -> none  [the longest x1 21.9 us: per_device(): lax.all_to_all(quarters[0], 'sp', split_axis=0, concat_axis=0, tiled=True)]
    all_gather x4 -> x2, waiting for transfers between devices: 58.1 us -> 39.7 us  [the longest x1 39.7 us: per_device(): normed_all = lax.all_gather(normed_bf, 'sp', axis=0, tiled=True)]
    gather x4 -> x0, local copies, waits for them, and re-layouts: 15.8 us -> none  [the longest x1 6.65 us: per_device(): jnp.take(pair_grad, picked, axis=0)]
    convert_element_type x15 -> x3, other arithmetic: 11.2 us -> 2.04 us  [the longest x1 1.28 us: per_device(): normed.transpose(1, 0, 2).reshape(tokens, heads * value_width).astype(BF16)]
  transfers between devices with their start and end apart: 7 -> 2, of which waited for: 5 -> 1; matrix products, arithmetic and copies ran while one was open for 11% -> 21% of each run, Pallas kernels for 0% -> 35%
where the time goes in v1:
time: 233 us
  Pallas kernels  112 us (48%)
  waiting for transfers between devices  39.7 us (17%)
  matrix products  36 us (15%)
  local copies, waits for them, and re-layouts  18.7 us (8%)
  between operations  14.8 us (6%)
  other arithmetic  11.7 us (5%)
    pallas_call x1, Pallas kernels, dispatch(): pl.pallas_call(functools.partial(dispatch_kernel, n_sp, n_tp, q), out_sha...  42.3 us
    all_gather x1, waiting for transfers between devices, per_device(): normed_all = lax.all_gather(normed_bf, 'sp', axis=0, tiled=True)  39.7 us
    pallas_call x1, Pallas kernels, give_back(): pl.pallas_call(functools.partial(return_kernel, n_sp, n_tp, q), out_shape...  38.7 us
    pallas_call x1, Pallas kernels, swap(): pl.pallas_call(functools.partial(swap_kernel, n_sp, w), out_shape=(jax.Sh...  30.7 us
    dot_general x9, matrix products, mm(): lax.dot_general(a, b, (((da,), (db,)), ((), ())), preferred_element_type=...  21.7 us
    unnamed x100, local copies, waits for them, and re-layouts  7.61 us
  transfers between devices with their start and end apart: 2, of which 1 were waited for; matrix products, arithmetic and copies ran while one was open for 21% of the time, Pallas kernels for 35%

profile of v1, /device:TPU:0, one launch (start us, length us, event | category | flops | bytes accessed | tf_op | source)
XLA Modules:
  0.0 232.7 jit_solution(2014548317299801039)
XLA Ops:
  7.3 0.9 copy.242
  9.0 1.0 copy.247
  10.0 0.6 broadcast_multiply_fusion.1
  10.6 0.9 fusion.78
  11.5 0.3 fusion.11
  11.8 1.7 convolution_convert_fusion.5
  13.6 0.5 pad.4
  14.2 0.6 iota_compare_fusion.9
  14.7 0.7 copy.264
  15.4 0.7 convert_reduce_fusion
  16.2 0.7 select_reduce_fusion
  17.0 0.7 convert_add_fusion
  17.8 1.3 slice_bitcast_fusion.5
  19.0 0.9 constant_dynamic-slice_fusion.og
  20.0 2.1 convolution_convert_fusion.3
  22.0 0.8 add_reduce_fusion
  22.8 1.1 fusion.4
  23.9 1.2 broadcast_in_dim.147.tot
  25.2 42.3 %dispatch.1 = (bf16[8,64,2048]{2,1,0:T(8,128)(2,1)}, bf16[8,64,2048]{2,1,0:T(8,128)(2,1)}, f32[8,8,128]{2,1,0:T(8,128)}) custom-call(bf16[8,64,512]{2,1,0:T(8,128)(2,1)} %bitcast.190, bf16[8,64,512]{2,1,0:T(8,128)(2,1)} %bitcast.197, f32[8,128]{1,0:T(8,128)} %broadcast_in_dim.147.tot), custom_call_target="tpu_custom_call" | custom-call | tf_op jit(solution)/shard_map/dispatch/pallas_call | solution.py:137
  67.5 2.5 %fusion.21 = f32[512,256]{1,0:T(8,128)S(1)} fusion(bf16[512,2048]{1,0:T(8,128)(2,1)} %bitcast.207, bf16[1,2048,256]{2,1,0:T(8,128)(2,1)S(1)} %copy-done.5), kind=kOutput, calls=%fused_computation.39 | convolution fusion | flops 536870912 | bytes 3670016 | tf_op jit(solution)/shard_map/dot_general | solution.py:346
  70.0 0.7 fusion.27
  70.8 1.2 copy-done.38
  72.0 0.3 copy-done.42
  72.2 1.7 select_convert_fusion
  73.9 0.7 copy-done.14
  74.6 2.7 %fusion.25 = f32[512,2048]{1,0:T(8,128)} fusion(bf16[512,256]{1,0:T(8,128)(2,1)S(1)} %get-tuple-element.64, bf16[1,2048,256]{2,1,0:T(8,128)(2,1)S(1)} %copy-done.4), kind=kOutput, calls=%fused_computation.43 | convolution fusion | flops 536870912 | bytes 5505024 | tf_op jit(solution)/shard_map/dot_general | solution.py:346
  77.3 0.7 copy.244
  78.1 4.4 %add_convert_fusion = bf16[512,2048]{1,0:T(8,128)(2,1)} fusion(f32[512,2048]{1,0:T(8,128)} %fusion.25, bf16[512,256]{1,0:T(8,128)(2,1)} %get-tuple-element.63, bf16[1,2048,256]{2,1,0:T(8,128)(2,1)S(1)} %copy-done.5), kind=kOutput, calls=%fused_computation | convolution fusion | flops 538968064 | bytes 7602176 | tf_op jit(solution)/shard_map/dot_general | solution.py:346
  82.5 0.8 fusion.39.comb
  83.2 38.7 %give_back.1.resid = bf16[128,2048]{1,0:T(8,128)(2,1)} custom-call(bf16[8,64,2048]{2,1,0:T(8,128)(2,1)} %bitcast.189, bf16[128,512]{1,0:T(8,128)(2,1)} %fusion.39.comb, bf16[128,512]{1,0:T(8,128)(2,1)} %copy-done.11), custom_call_target="tpu_custom_call" | custom-call | tf_op jit(solution)/shard_map/give_back/pallas_call | solution.py:246
  122.1 2.0 fusion.93
  124.2 0.8 slice.33
  125.5 0.7 copy.255
  126.2 0.6 copy.259
  126.8 0.7 copy.268
  127.6 0.7 copy.272
  128.2 0.7 copy.271
  129.0 0.3 fusion.9
  129.3 0.4 convolution_multiply_fusion.2
  129.7 3.5 %fusion = bf16[1,2048,256]{2,1,0:T(8,128)(2,1)} fusion(bf16[512,2048]{1,0:T(8,128)(2,1)} %bitcast.208, bf16[512,256]{1,0:T(8,128)(2,1)S(1)} %copy-done.15), kind=kOutput, calls=%fused_computation.4 | convolution fusion | flops 537395200 | bytes 3407872 | tf_op jit(solution)/shard_map/dot_general | solution.py:346
  133.2 1.8 fusion.1
  135.0 0.4 copy-done.46
  135.4 1.8 fusion.2
  137.2 1.5 fusion.3
  138.7 0.4 fusion.92
  139.2 1.0 multiply_reduce_fusion.1
  140.2 0.6 fusion.89
  141.1 0.8 convolution_convert_fusion.4.state
  141.9 0.3 fusion.19
  142.2 30.7 %swap.1 = (bf16[8,128,256]{2,1,0:T(8,128)(2,1)}, bf16[8,2,128,256]{3,2,1,0:T(8,128)(2,1)}) custom-call(bf16[128,2048]{1,0:T(8,128)(2,1)} %give_back.1.resid, bf16[2,128,256]{2,1,0:T(8,128)(2,1)} %convolution_convert_fusion.4.state), custom_call_target="tpu_custom_call" | custom-call | tf_op jit(solution)/shard_map/swap/pallas_call | solution.py:302
  172.9 1.3 fusion.31
  174.2 0.8 copy.260
  175.2 0.8 copy.266
  176.0 0.4 fusion.95
  176.5 1.2 fusion.17
  177.7 0.7 copy.279
  178.4 1.5 multiply_reduce_fusion
  180.4 1.1 fusion.18
  181.6 0.7 copy.280
  182.3 0.2 convolution_bitcast_fusion.1
  182.5 0.2 fusion.7
  182.7 0.8 copy.281
  183.5 39.7 %all-gather.4.cloned.1.call-done = bf16[1024,512]{0,1:T(8,128)(2,1)} async-done(((bf16[128,512]{0,1:T(8,128)(2,1)}), bf16[1024,512]{0,1:T(8,128)(2,1)}) %all-gather.4.cloned.1.call-update) | async-done | bytes 1048592 | tf_op jit(solution)/shard_map/all_gather | solution.py:464
  223.2 2.7 %fusion.94 = f32[256,512]{1,0:T(8,128)} fusion(bf16[1024,256]{1,0:T(8,128)(2,1)} %bitcast.199, bf16[1024,512]{0,1:T(8,128)(2,1)} %all-gather.4.cloned.1.call-done), kind=kOutput, calls=%fused_computation.166 | convolution fusion | flops 268435456 | bytes 2097152 | tf_op jit(solution)/shard_map/dot_general | solution.py:346
  (123 shorter events, 3.0 us)
Async XLA Ops:
  7.2 114.8 %copy-start = (bf16[2048,512]{1,0:T(8,128)(2,1)S(1)}, bf16[2048,512]{1,0:T(8,128)(2,1)}, u32[]{:S(2)}) copy-start(bf16[2048,512]{1,0:T(8,128)(2,1)} %param.20) | copy-start | bytes 6291460
  7.2 130.0 %all-gather.6.cloned.1.call-start = ((), (), s32[]{:S(2)}) async-start(), calls=%async_computation.1 | async-start | bytes 1179648 | tf_op jit(solution)/shard_map/all_gather | solution.py:438
  7.3 10.4 %copy-start.26 = (s32[128]{0:T(128)}, s32[128]{0:T(128)S(1)}, u32[]{:S(2)}) copy-start(s32[128]{0:T(128)S(1)} %get-tuple-element.84) | copy-start | bytes 1540
  7.3 10.4 %copy-start.29 = (s32[128]{0:T(128)}, s32[128]{0:T(128)S(1)}, u32[]{:S(2)}) copy-start(s32[128]{0:T(128)S(1)} %get-tuple-element.85) | copy-start | bytes 1540
  7.3 10.4 %copy-start.32 = (pred[128]{0:T(512)(128)(4,1)}, pred[128]{0:T(512)(128)(4,1)S(1)}, u32[]{:S(2)}) copy-start(pred[128]{0:T(512)(128)(4,1)S(1)} %get-tuple-element.80) | copy-start | bytes 388
  7.3 10.4 %copy-start.34 = (pred[128]{0:T(512)(128)(4,1)}, pred[128]{0:T(512)(128)(4,1)S(1)}, u32[]{:S(2)}) copy-start(pred[128]{0:T(512)(128)(4,1)S(1)} %get-tuple-element.81) | copy-start | bytes 388
  8.4 1.6 copy-start.6
  8.5 9.2 %copy-start.18 = (f32[128,2]{0,1:T(2,128)}, f32[128,2]{0,1:T(2,128)S(1)}, u32[]{:S(2)}) copy-start(f32[128,2]{0,1:T(2,128)S(1)} %copy.243) | copy-start | bytes 3076
  11.5 56.0 %copy-start.5 = (bf16[1,2048,256]{2,1,0:T(8,128)(2,1)S(1)}, bf16[1,2048,256]{2,1,0:T(8,128)(2,1)}, u32[]{:S(2)}) copy-start(bf16[1,2048,256]{2,1,0:T(8,128)(2,1)} %param.22) | copy-start | bytes 3145732
  13.6 209.6 %all-gather.4.cloned.1.call-start = ((), (), s32[]{:S(2)}) async-start(), calls=%async_computation | async-start | bytes 1179648 | tf_op jit(solution)/shard_map/all_gather | solution.py:464
  20.0 4.0 %copy-start.11 = (bf16[128,512]{1,0:T(8,128)(2,1)}, bf16[128,512]{1,0:T(8,128)(2,1)S(1)}, u32[]{:S(2)}) copy-start(bf16[128,512]{1,0:T(8,128)(2,1)S(1)} %constant_dynamic-slice_fusion.og) | copy-start | bytes 393220
  67.5 2.5 %copy-start.4 = (bf16[1,2048,256]{2,1,0:T(8,128)(2,1)S(1)}, bf16[1,2048,256]{2,1,0:T(8,128)(2,1)}, u32[]{:S(2)}) copy-start(bf16[1,2048,256]{2,1,0:T(8,128)(2,1)} %param.21) | copy-start | bytes 3145732
  67.5 2.5 %copy-start.40 = (bf16[8,64,2048]{2,1,0:T(8,128)(2,1)S(1)}, bf16[8,64,2048]{2,1,0:T(8,128)(2,1)}, u32[]{:S(2)}) copy-start(bf16[8,64,2048]{2,1,0:T(8,128)(2,1)} %get-tuple-element.12) | copy-start | bytes 6291460
  70.0 3.9 %copy-start.43 = (f32[512,256]{1,0:T(8,128)}, f32[512,256]{1,0:T(8,128)S(1)}, u32[]{:S(2)}) copy-start(f32[512,256]{1,0:T(8,128)S(1)} %fusion.21) | copy-start | bytes 1572868
  70.0 2.0 copy-start.38
  70.0 2.2 copy-start.42
  70.7 3.2 %copy-start.45 = (f32[512,256]{1,0:T(8,128)}, f32[512,256]{1,0:T(8,128)S(1)}, u32[]{:S(2)}) copy-start(f32[512,256]{1,0:T(8,128)S(1)} %fusion.27) | copy-start | bytes 1572868
  73.9 0.7 copy-start.14
  74.6 2.7 %copy-start.17 = (bf16[128,2,128]{2,1,0:T(2,128)(2,1)S(1)}, bf16[128,2,128]{2,1,0:T(2,128)(2,1)}, u32[]{:S(2)}) copy-start(bf16[128,2,128]{2,1,0:T(2,128)(2,1)} %param.16) | copy-start | bytes 196612
  122.0 3.3 %copy-start.36 = (pred[8]{0:T(512)(128)(4,1)S(1)}, pred[8]{0:T(512)(128)(4,1)}, u32[]{:S(2)}) copy-start(pred[8]{0:T(512)(128)(4,1)} %get-tuple-element.83) | copy-start | bytes 28
  122.0 3.4 %copy-start.37 = (pred[8]{0:T(512)(128)(4,1)S(1)}, pred[8]{0:T(512)(128)(4,1)}, u32[]{:S(2)}) copy-start(pred[8]{0:T(512)(128)(4,1)} %get-tuple-element.82) | copy-start | bytes 28
  122.0 4.2 %copy-start.7 = (f32[128,2]{1,0:T(8,128)S(1)}, f32[128,2]{1,0:T(8,128)}, u32[]{:S(2)}) copy-start(f32[128,2]{1,0:T(8,128)} %copy-done.6) | copy-start | bytes 3076
  122.0 4.8 %copy-start.12 = (f32[128,128]{0,1:T(8,128)S(1)}, f32[128,128]{0,1:T(8,128)}, u32[]{:S(2)}) copy-start(f32[128,128]{0,1:T(8,128)} %get-tuple-element.69) | copy-start | bytes 196612
  122.0 6.9 %copy-start.13 = (bf16[128,2,128]{0,2,1:T(8,128)(2,1)S(1)}, bf16[128,2,128]{0,2,1:T(8,128)(2,1)}, u32[]{:S(2)}) copy-start(bf16[128,2,128]{0,2,1:T(8,128)(2,1)} %copy.244) | copy-start | bytes 196612
  122.0 6.9 %copy-start.27 = (s32[128]{0:T(128)S(1)}, s32[128]{0:T(128)}, u32[]{:S(2)}) copy-start(s32[128]{0:T(128)} %copy-done.26) | copy-start | bytes 1540
  122.0 6.9 %copy-start.30 = (s32[128]{0:T(128)S(1)}, s32[128]{0:T(128)}, u32[]{:S(2)}) copy-start(s32[128]{0:T(128)} %copy-done.29) | copy-start | bytes 1540
  122.0 6.9 %copy-start.33 = (pred[128]{0:T(512)(128)(4,1)S(1)}, pred[128]{0:T(512)(128)(4,1)}, u32[]{:S(2)}) copy-start(pred[128]{0:T(512)(128)(4,1)} %copy-done.32) | copy-start | bytes 388
  122.1 6.9 %copy-start.35 = (pred[128]{0:T(512)(128)(4,1)S(1)}, pred[128]{0:T(512)(128)(4,1)}, u32[]{:S(2)}) copy-start(pred[128]{0:T(512)(128)(4,1)} %copy-done.34) | copy-start | bytes 388
  122.1 7.2 %copy-start.19 = (f32[128,2]{0,1:T(2,128)S(1)}, f32[128,2]{0,1:T(2,128)}, u32[]{:S(2)}) copy-start(f32[128,2]{0,1:T(2,128)} %copy-done.18) | copy-start | bytes 3076
  122.1 7.6 %copy-start.15 = (bf16[512,256]{1,0:T(8,128)(2,1)S(1)}, bf16[512,256]{1,0:T(8,128)(2,1)}, u32[]{:S(2)}) copy-start(bf16[512,256]{1,0:T(8,128)(2,1)} %copy-done.14) | copy-start | bytes 786436
  129.7 9.5 %copy-start.2 = (f32[2,128,128]{2,1,0:T(8,128)}, f32[2,128,128]{2,1,0:T(8,128)S(1)}, u32[]{:S(2)}) copy-start(f32[2,128,128]{2,1,0:T(8,128)S(1)} %convolution_multiply_fusion.2) | copy-start | bytes 393220
  129.7 3.5 %copy-start.16 = (bf16[512,256]{1,0:T(8,128)(2,1)S(1)}, bf16[512,256]{1,0:T(8,128)(2,1)}, u32[]{:S(2)}) copy-start(bf16[512,256]{1,0:T(8,128)(2,1)} %get-tuple-element.63) | copy-start | bytes 786436
  129.7 3.5 %copy-start.41 = (bf16[8,64,2048]{2,1,0:T(8,128)(2,1)S(1)}, bf16[8,64,2048]{2,1,0:T(8,128)(2,1)}, u32[]{:S(2)}) copy-start(bf16[8,64,2048]{2,1,0:T(8,128)(2,1)} %get-tuple-element.12) | copy-start | bytes 6291460
  133.2 1.8 copy-start.39
  133.2 1.8 copy-start.44
  133.2 2.1 copy-start.46
  135.4 1.8 copy-start.22
  135.4 3.8 %copy-start.1 = (bf16[128,2,256]{2,1,0:T(2,128)(2,1)S(1)}, bf16[128,2,256]{2,1,0:T(2,128)(2,1)}, u32[]{:S(2)}) copy-start(bf16[128,2,256]{2,1,0:T(2,128)(2,1)} %param.18) | copy-start | bytes 393220
  135.4 3.8 %copy-start.23 = (f32[2,128]{1,0:T(2,128)S(1)}, f32[2,128]{1,0:T(2,128)}, u32[]{:S(2)}) copy-start(f32[2,128]{1,0:T(2,128)} %get-tuple-element.74) | copy-start | bytes 3076
  137.2 3.9 %copy-start.24 = (f32[2,128]{1,0:T(2,128)S(1)}, f32[2,128]{1,0:T(2,128)}, u32[]{:S(2)}) copy-start(f32[2,128]{1,0:T(2,128)} %get-tuple-element.74) | copy-start | bytes 3076
  138.7 3.2 %copy-start.20 = (f32[128,2]{0,1:T(2,128)S(1)}, f32[128,2]{0,1:T(2,128)}, u32[]{:S(2)}) copy-start(f32[128,2]{0,1:T(2,128)} %copy-done.18) | copy-start | bytes 3076
  142.2 33.0 %copy-start.8 = (bf16[2,128,128]{2,1,0:T(8,128)(2,1)}, bf16[2,128,128]{2,1,0:T(8,128)(2,1)S(1)}, u32[]{:S(2)}) copy-start(bf16[2,128,128]{2,1,0:T(8,128)(2,1)S(1)} %fusion.19) | copy-start | bytes 196612
  142.2 36.2 %copy-start.21 = (f32[8,2]{1,0:T(8,128)S(1)}, f32[8,2]{1,0:T(8,128)}, u32[]{:S(2)}) copy-start(f32[8,2]{1,0:T(8,128)} %copy.272) | copy-start | bytes 196
  175.0 5.4 %copy-start.10 = (f32[128,128]{1,0:T(8,128)S(1)}, f32[128,128]{1,0:T(8,128)}, u32[]{:S(2)}) copy-start(f32[128,128]{1,0:T(8,128)} %copy.264) | copy-start | bytes 196612
  175.0 5.4 %copy-start.25 = (f32[128,2]{0,1:T(2,128)S(1)}, f32[128,2]{0,1:T(2,128)}, u32[]{:S(2)}) copy-start(f32[128,2]{0,1:T(2,128)} %copy.271) | copy-start | bytes 3076
  175.0 5.4 %copy-start.28 = (s32[128]{0:T(128)S(1)}, s32[128]{0:T(128)}, u32[]{:S(2)}) copy-start(s32[128]{0:T(128)} %copy-done.26) | copy-start | bytes 1540
  175.0 5.4 %copy-start.31 = (s32[128]{0:T(128)S(1)}, s32[128]{0:T(128)}, u32[]{:S(2)}) copy-start(s32[128]{0:T(128)} %copy-done.29) | copy-start | bytes 1540
  176.0 4.0 %copy-start.9 = (bf16[2,128,128]{2,1,0:T(8,128)(2,1)S(1)}, bf16[2,128,128]{2,1,0:T(8,128)(2,1)}, u32[]{:S(2)}) copy-start(bf16[2,128,128]{2,1,0:T(8,128)(2,1)} %copy-done.8) | copy-start | bytes 196612
  176.0 6.3 %copy-start.3 = (f32[2,128,128]{2,1,0:T(8,128)S(1)}, f32[2,128,128]{2,1,0:T(8,128)}, u32[]{:S(2)}) copy-start(f32[2,128,128]{2,1,0:T(8,128)} %copy-done.2) | copy-start | bytes 393220
Sparse Core Ops, SparseCore 0:
  13.7 55.1 all-gather.5
  175.1 48.0 all-gather.3

commit v2 on v1

--- a/solution.py
+++ b/solution.py
@@ -55,9 +55,95 @@
     )
 
 
+class Chain:
+    def __init__(self, src, out, n_sp, me, c, sems, ways):
+        self.src, self.out, self.me, self.c = src, out, me, c
+        self.pairs, self.ways = n_sp // 2, ways
+        self.pair = me // 2
+        self.other = me + 1 - 2 * lax.rem(me, 2)
+        self.zs, self.zr, self.ys, self.yr, self.own_sem = sems
+
+    def has(self, d, way):
+        return self.pair >= d if way == 0 else self.pair + d < self.pairs
+
+    def room(self, way):
+        return self.pair + 1 < self.pairs if way == 0 else self.pair >= 1
+
+    def spot(self, base, d, way):
+        return self.out.at[base - 2 * d if way == 0 else base + 2 * d]
+
+    def along(self, d, way):
+        spot = self.spot(self.me, d, way)
+        return push(
+            self.src if d == 0 else spot, spot, self.zs.at[way, d], self.zr.at[way, d + 1],
+            (self.me + 2 if way == 0 else self.me - 2, self.c),
+        )
+
+    def across(self, d, way):
+        spot = self.spot(self.me, d, way)
+        return push(
+            self.src if d == 0 else spot, spot, self.ys.at[way, d], self.yr.at[way, d],
+            (self.other, self.c),
+        )
+
+    def own(self):
+        return pltpu.make_async_copy(self.src, self.out.at[self.me], self.own_sem.at[0])
+
+    def each(self, d, act):
+        for way in self.ways:
+
+            @pl.when(self.has(d, way))
+            def _():
+                if d < self.pairs - 1:
+
+                    @pl.when(self.room(way))
+                    def _():
+                        act(self.along(d, way))
+
+                if d > 0 or way == self.ways[0]:
+                    act(self.across(d, way))
+
+    def start(self):
+        self.own().start()
+        self.each(0, lambda cp: cp.start())
+
+    def step(self, d):
+        for way in self.ways:
+
+            @pl.when(self.has(d, way))
+            def _():
+                spot = self.spot(self.me, d, way)
+                push(
+                    spot, spot, self.zs.at[way, d], self.zr.at[way, d], (self.other, self.c)
+                ).wait_recv()
+
+        self.each(d, lambda cp: cp.start())
+
+    def finish(self):
+        for d in range(self.pairs):
+            for way in self.ways:
+                if d == 0 and way != self.ways[0]:
+                    continue
+
+                @pl.when(self.has(d, way))
+                def _():
+                    spot = self.spot(self.other, d, way)
+                    push(
+                        spot, spot, self.ys.at[way, d], self.yr.at[way, d], (self.other, self.c)
+                    ).wait_recv()
+
+            self.each(d, lambda cp: cp.wait_send())
+        self.own().wait()
+
+
+def chain_sems(n_sp):
+    dma = pltpu.SemaphoreType.DMA
+    return [dma((2, n_sp // 2))] * 4 + [dma((1,))]
+
+
 def dispatch_kernel(
-    n_sp, n_tp, q, rows, grads, tot, rows_out, grads_out, tot_out,
-    own_sem, ssem, rsem, xssem, xrsem, dssem, drsem, essem, ersem, tssem, trsem,
+    n_sp, n_tp, q, rows, grads, tot, state, rows_out, grads_out, tot_out, states,
+    own_sem, ssem, rsem, xssem, xrsem, dssem, drsem, essem, ersem, tssem, trsem, *chain_sem,
 ):
     me = lax.axis_index("sp")
     c = lax.axis_index("tp")
@@ -68,6 +154,8 @@
     def cols(quarter):
         return pl.ds(pl.multiple_of(quarter * q, 128), q)
 
+    chain = Chain(state, states, n_sp, me, c, chain_sem, (0,))
+    chain.start()
     waits = []
     for k in range(1, n_sp):
         peer = lax.rem(me + k, n_sp)
@@ -113,6 +201,8 @@
                 sent.append(cp)
         if k >= 1:
             relay(k - 1)
+        if k and k % 2 == 0:
+            chain.step(k // 2)
     relay(n_sp - 1)
     near_far = lax.rem(near + n_tp // 2, n_tp)
     for out, source, a, k in last:
@@ -128,27 +218,33 @@
         cp.wait_send()
     for cp in local:
         cp.wait()
-
-
-def dispatch(rows, grads, tot, n_tp):
+    chain.finish()
+
+
+def dispatch(rows, grads, tot, state, n_tp):
     n_sp, cap, q = rows.shape
     full = jax.ShapeDtypeStruct((n_sp, cap, q * n_tp), rows.dtype)
     dma = pltpu.SemaphoreType.DMA
     return pl.pallas_call(
         functools.partial(dispatch_kernel, n_sp, n_tp, q),
-        out_shape=(full, full, jax.ShapeDtypeStruct((n_sp,) + tot.shape, tot.dtype)),
-        in_specs=any_specs(3),
-        out_specs=tuple(any_specs(3)),
-        scratch_shapes=[dma((3,))] + [dma((2, n_sp))] * 8 + [dma((n_sp,))] * 2,
+        out_shape=(
+            full,
+            full,
+            jax.ShapeDtypeStruct((n_sp,) + tot.shape, tot.dtype),
+            jax.ShapeDtypeStruct((n_sp,) + state.shape, state.dtype),
+        ),
+        in_specs=any_specs(4),
+        out_specs=tuple(any_specs(4)),
+        scratch_shapes=[dma((3,))] + [dma((2, n_sp))] * 8 + [dma((n_sp,))] * 2 + chain_sems(n_sp),
         compiler_params=pltpu.CompilerParams(collective_id=0, has_side_effects=True),
         name="dispatch",
-    )(rows, grads, tot)
+    )(rows, grads, tot, state)
 
 
 def return_kernel(
-    n_sp, n_tp, q, back, comb, og, resid,
+    n_sp, n_tp, q, back, comb, og, normed, resid, normed_all,
     part, xbuf, xrecv, sendbuf, ret, resq,
-    pssem, prsem, xssem, xrsem, ssem, rsem, gssem, grsem,
+    pssem, prsem, xssem, xrsem, ssem, rsem, gssem, grsem, *chain_sem,
 ):
     me = lax.axis_index("sp")
     c = lax.axis_index("tp")
@@ -170,6 +266,8 @@
             )
             cp.start()
             waits.append(cp)
+    chain = Chain(normed, normed_all, n_sp, me, c, chain_sem, (0, 1))
+    chain.start()
 
     def to_far(k):
         cp = push(xbuf.at[k], xrecv.at[k], xssem.at[k], xrsem.at[k], (me, far))
@@ -210,6 +308,8 @@
             second(order[n - lag])
         if n >= lag + 1 and order[n - lag - 1] != 0:
             to_home(order[n - lag - 1])
+        if n and n % 2 == 0 and n < n_sp:
+            chain.step(n // 2)
     for k in range(1, n_sp):
         source = lax.rem(me + n_sp - k, n_sp)
         push(sendbuf.at[k], ret.at[source], ssem.at[k], rsem.at[k], (me, far)).wait_recv()
@@ -235,9 +335,10 @@
     own.wait()
     for cp in waits:
         cp.wait_send()
-
-
-def give_back(back, comb, og_q, n_tp):
+    chain.finish()
+
+
+def give_back(back, comb, og_q, normed, n_tp):
     n_sp, cap, width = back.shape
     q = width // n_tp
     tokens = og_q.shape[0]
@@ -245,21 +346,25 @@
     block = pltpu.VMEM((n_sp, cap, q), BF16)
     return pl.pallas_call(
         functools.partial(return_kernel, n_sp, n_tp, q),
-        out_shape=jax.ShapeDtypeStruct((tokens, width), BF16),
-        in_specs=vmem_specs(3),
-        out_specs=pl.BlockSpec(memory_space=pl.ANY),
+        out_shape=(
+            jax.ShapeDtypeStruct((tokens, width), BF16),
+            jax.ShapeDtypeStruct((n_sp,) + normed.shape, BF16),
+        ),
+        in_specs=vmem_specs(3) + any_specs(1),
+        out_specs=tuple(any_specs(2)),
         scratch_shapes=[pltpu.VMEM((2, n_sp, cap, q), BF16)]
         + [block] * 4
         + [pltpu.VMEM((tokens, q), BF16)]
         + [dma((2, n_sp))] * 2
         + [dma((n_sp,))] * 4
-        + [dma((4,)), dma((3,))],
+        + [dma((4,)), dma((3,))]
+        + chain_sems(n_sp),
         compiler_params=pltpu.CompilerParams(collective_id=1, has_side_effects=True),
         name="give_back",
-    )(back, comb, og_q)
-
-
-def swap_kernel(n_sp, w, resid, state, cols_out, states, own_sem, ssem, rsem):
+    )(back, comb, og_q, normed)
+
+
+def swap_kernel(n_sp, w, resid, state, cols_out, states, own_sem, ssem, rsem, *chain_sem):
     me = lax.axis_index("sp")
     c = lax.axis_index("tp")
     greet(n_sp, me, c, True, ())
@@ -269,28 +374,26 @@
             return resid.at[index]
         return resid.at[:, pl.ds(pl.multiple_of(index * w, 128), w)]
 
+    chain = Chain(state, states, n_sp, me, c, chain_sem, (1,))
+    chain.start()
     waits = []
     for k in range(1, n_sp):
         peer = lax.rem(me + k, n_sp)
-        for a, (src, out) in enumerate(((state, states), (part(peer), cols_out))):
-            cp = push(src, out.at[me], ssem.at[a, k], rsem.at[a, k], (peer, c))
-            cp.start()
-            waits.append(cp)
-    local = [
-        pltpu.make_async_copy(part(me), cols_out.at[me], own_sem.at[0]),
-        pltpu.make_async_copy(state, states.at[me], own_sem.at[1]),
-    ]
-    for cp in local:
+        cp = push(part(peer), cols_out.at[me], ssem.at[k], rsem.at[k], (peer, c))
         cp.start()
+        waits.append(cp)
+    local = pltpu.make_async_copy(part(me), cols_out.at[me], own_sem.at[0])
+    local.start()
+    for d in range(1, n_sp // 2):
+        chain.step(d)
     for k in range(1, n_sp):
         source = lax.rem(me + n_sp - k, n_sp)
-        for a, out in enumerate((states, cols_out)):
-            spot = out.at[source]
-            push(spot, spot, ssem.at[a, k], rsem.at[a, k], (source, c)).wait_recv()
+        spot = cols_out.at[source]
+        push(spot, spot, ssem.at[k], rsem.at[k], (source, c)).wait_recv()
     for cp in waits:
         cp.wait_send()
-    for cp in local:
-        cp.wait()
+    local.wait()
+    chain.finish()
 
 
 def swap(resid, state, n_sp):
@@ -307,7 +410,7 @@
         ),
         in_specs=any_specs(2),
         out_specs=tuple(any_specs(2)),
-        scratch_shapes=[dma((2,)), dma((2, n_sp)), dma((2, n_sp))],
+        scratch_shapes=[dma((1,)), dma((n_sp,)), dma((n_sp,))] + chain_sems(n_sp),
         compiler_params=pltpu.CompilerParams(collective_id=2, has_side_effects=True),
         name="swap",
     )(resid, state)
@@ -340,6 +443,11 @@
 
 def fine(spec, a, b):
     return jnp.einsum(spec, a.astype(F32), b.astype(F32), precision=lax.Precision.HIGHEST)
+
+
+def weighted(states, factors, present):
+    kept = jnp.where(present[:, None, None, None], states.astype(F32), 0.0)
+    return jnp.sum(kept * factors[:, :, None, None], axis=0)
 
 
 def mm(a, b, da, db):
@@ -416,13 +524,6 @@
     running = jnp.cumsum(log_decay, axis=0).T
     block_total = running[:, -1]
     tot = jnp.broadcast_to(jnp.pad(block_total, (0, 128 - heads))[None, :], (8, 128))
-    rows, grads, tots = dispatch(
-        send_rows.reshape(n_sp, capacity, quarter),
-        send_grads.reshape(n_sp, capacity, quarter),
-        tot,
-        n_tp,
-    )
-
     matrix = swap_matrix(key_width)
     cosines, sines = rotation_tables(me * tokens, tokens, key_width)
     scale = key_width ** (-0.5)
@@ -435,7 +536,13 @@
     decay = jnp.exp(running)[..., None]
     remaining = jnp.exp(block_total[:, None] - running)[..., None]
     inner = ein("wfs,wfi->wsi", key_rot * remaining, values).astype(BF16)
-    inner_all = lax.all_gather(inner, "sp")
+    rows, grads, tots, inner_all = dispatch(
+        send_rows.reshape(n_sp, capacity, quarter),
+        send_grads.reshape(n_sp, capacity, quarter),
+        tot,
+        inner,
+        n_tp,
+    )
     key_bf = key_rot.astype(BF16)
     query_bf = query_rot.astype(BF16)
     weights = fine("hik,hjk->hij", query_rot, key_rot) * mask
@@ -456,14 +563,15 @@
     past = jnp.where((ids < me)[:, None], jnp.exp(past), 0.0)
     coming = jnp.where((ids > me)[:, None], sums - totals - sum_through[None], 0.0)
     coming = jnp.where((ids > me)[:, None], jnp.exp(coming), 0.0)
-    incoming = jnp.sum(inner_all.astype(F32) * past[:, :, None, None], axis=0)
+    incoming = weighted(inner_all, past, ids < me)
     retained = retained_local + decay * fine("dzr,drs->dzs", query_rot, incoming)
     inverse_rms = lax.rsqrt(jnp.mean(retained * retained, axis=-1, keepdims=True) + EPSILON)
     normed = retained * inverse_rms
     normed_bf = normed.transpose(1, 0, 2).reshape(tokens, heads * value_width).astype(BF16)
-    normed_all = lax.all_gather(normed_bf, "sp", axis=0, tiled=True)
-
-    resid = give_back(back_rows.reshape(n_sp, capacity, width), comb, og_q, n_tp)
+
+    resid, normed_all = give_back(
+        back_rows.reshape(n_sp, capacity, width), comb, og_q, normed_bf, n_tp
+    )
     normed_grad = jnp.dot(resid, out_proj, preferred_element_type=F32)
     normed_grad = normed_grad.reshape(tokens, heads, value_width).transpose(1, 0, 2)
     grad = inverse_rms * (
@@ -472,7 +580,7 @@
     grad_bf = grad.astype(BF16)
     inner_grad = ein("gwn,gwj->gnj", query_rot * decay, grad_bf).astype(BF16)
     resid_cols, grads_all = swap(resid, inner_grad, n_sp)
-    future = jnp.sum(grads_all.astype(F32) * coming[:, :, None, None], axis=0).astype(BF16)
+    future = weighted(grads_all, coming, ids > me).astype(BF16)
     score = fine("hiv,hjv->hij", grad, values) * mask
     query_portion = ein("hij,hjk->hik", score, key_bf) + decay * fine(
         "bpl,btl->bpt", grad, incoming
@@ -488,7 +596,9 @@
         (turn(key_portion, cosines, -sines, matrix) * scale).astype(BF16).transpose(1, 0, 2)
     )
     value_grad = value_portion.astype(BF16).transpose(1, 0, 2)
-    proj_grad = mm(resid_cols.reshape(n_sp * tokens, -1), normed_all, 0, 0)
+    proj_grad = mm(
+        resid_cols.reshape(n_sp * tokens, -1), normed_all.reshape(n_sp * tokens, -1), 0, 0
+    )
     return (
         gate_part[None],
         up_part[None],

time: 233 us -> 172 us (0.74)
  waiting for transfers between devices: 39.7 us -> 0 us
  between operations: 14.8 us -> 1.18 us
  matrix products: 36 us -> 28.6 us
  Pallas kernels: 112 us -> 118 us
  local copies, waits for them, and re-layouts: 18.7 us -> 13.9 us
  other arithmetic: 11.7 us -> 9.13 us
    all_gather x2 -> x0, waiting for transfers between devices: 39.7 us -> none  [the longest x1 39.7 us: per_device(): normed_all = lax.all_gather(normed_bf, 'sp', axis=0, tiled=True)]
    pallas_call x1, Pallas kernels: 38.7 us -> 47.4 us  [give_back(): pl.pallas_call(functools.partial(return_kernel, n_sp, n_tp, q), out_shape...]
    dot_general x9, matrix products: 21.7 us -> 15.3 us  [mm(): lax.dot_general(a, b, (((da,), (db,)), ((), ())), preferred_element_type=...]
    unnamed x100 -> x58, local copies, waits for them, and re-layouts: 7.61 us -> 6.61 us
  transfers between devices with their start and end apart: 2 -> 0, of which waited for: 1 -> 0; matrix products, arithmetic and copies ran while one was open for 21% -> 0% of each run, Pallas kernels for 35% -> 0%
where the time goes in v2:
time: 172 us; the launch traced here: 171 us
  Pallas kernels  118 us (69%)
  matrix products  28.6 us (17%)
  local copies, waits for them, and re-layouts  13.9 us (8%)
  other arithmetic  9.13 us (5%)
    pallas_call x1, Pallas kernels, give_back(): pl.pallas_call(functools.partial(return_kernel, n_sp, n_tp, q), out_shape...  47.4 us
    pallas_call x1, Pallas kernels, dispatch(): pl.pallas_call(functools.partial(dispatch_kernel, n_sp, n_tp, q), out_sha...  40.5 us
    pallas_call x1, Pallas kernels, swap(): pl.pallas_call(functools.partial(swap_kernel, n_sp, w), out_shape=(jax.Sh...  30.3 us
    dot_general x9, matrix products, mm(): lax.dot_general(a, b, (((da,), (db,)), ((), ())), preferred_element_type=...  15.3 us
    unnamed x58, local copies, waits for them, and re-layouts  6.61 us

profile of v2, /device:TPU:0, one launch (start us, length us, event | category | flops | bytes accessed | tf_op | source)
XLA Modules:
  0.0 171.1 jit_solution(13984169700648233050)
XLA Ops:
  0.8 0.8 slice_bitcast_fusion.5
  1.7 0.7 convert_reduce_fusion
  2.5 0.7 select_reduce_fusion
  3.2 0.7 convert_add_fusion
  4.0 0.1 mul.299
  4.1 1.0 copy.206
  5.1 1.0 copy.202
  6.1 0.8 copy.200
  6.9 0.2 reduce_window_sum.22
  7.1 0.2 slice_reduce_fusion
  7.3 0.7 broadcast_multiply_fusion.1
  8.0 0.6 broadcast_in_dim.167.tot
  8.6 0.7 copy.230
  9.3 0.8 fusion.38.comb
  10.2 0.2 add_reduce_fusion
  10.4 0.9 constant_dynamic-slice_fusion.og
  11.3 0.3 fusion.78
  11.7 0.3 fusion.10
  12.0 0.3 fusion.8
  12.5 0.8 convolution_convert_fusion.5.state
  13.3 0.4 convolution_multiply_fusion.2
  13.7 1.1 fusion.3
  14.8 2.0 %convolution_convert_fusion.3 = bf16[512,512]{1,0:T(8,128)(2,1)} fusion(bf16[128,2048]{1,0:T(8,128)(2,1)} %param.12, s32[]{:T(128)S(6)} %select_n.92, pred[2,512,128]{2,1,0:T(32,128)(4,1)S(1)} %iota_compare_fusion), kind=kOutput, calls=%fused_computation.11 | convolution fusion | flops 67436544 | bytes 786436 | tf_op jit(solution)/shard_map/dot_general | solution.py:519
  16.8 40.5 %dispatch.1 = (bf16[8,64,2048]{2,1,0:T(8,128)(2,1)}, bf16[8,64,2048]{2,1,0:T(8,128)(2,1)}, f32[8,8,128]{2,1,0:T(8,128)}, bf16[8,2,128,256]{3,2,1,0:T(8,128)(2,1)}) custom-call(bf16[8,64,512]{2,1,0:T(8,128)(2,1)} %bitcast.195, bf16[8,64,512]{2,1,0:T(8,128)(2,1)} %bitcast.202, f32[8,128]{1,0:T(8,128)} %broadcast_in_dim.167.tot, ...), custom_call_target="tpu_custom_call" | custom-call | tf_op jit(solution)/shard_map/dispatch/pallas_call | solution.py:228
  57.3 0.8 slice.33
  58.3 0.2 reduce_window_sum.23
  58.6 0.7 copy.231
  59.3 1.6 multiply_reduce_fusion.1
  61.0 0.4 fusion.92
  61.4 2.8 %fusion.20 = f32[512,256]{1,0:T(8,128)S(1)} fusion(bf16[512,2048]{1,0:T(8,128)(2,1)} %bitcast.208, bf16[1,2048,256]{2,1,0:T(8,128)(2,1)} %param.22), kind=kOutput, calls=%fused_computation.39 | convolution fusion | flops 536870912 | bytes 3670016 | tf_op jit(solution)/shard_map/dot_general | solution.py:454
  64.2 0.7 fusion.26
  65.0 0.9 copy-done.24
  65.8 0.3 copy-done.25
  66.1 1.0 select_convert_fusion
  67.1 1.8 %fusion.2 = bf16[1,256,2048]{2,1,0:T(8,128)(2,1)} fusion(bf16[512,2048]{1,0:T(8,128)(2,1)S(1)} %bitcast.213, f32[512,256]{1,0:T(8,128)S(1)} %fusion.26, f32[512,256]{1,0:T(8,128)S(1)} %fusion.20), kind=kOutput, calls=%fused_computation.6 | convolution fusion | flops 538705920 | bytes 4194304 | tf_op jit(solution)/shard_map/dot_general | solution.py:454
  68.9 0.3 multiply_reduce_fusion.2
  69.2 0.6 add_rsqrt_fusion
  70.0 0.7 copy.263
  70.6 1.8 %fusion.1 = bf16[1,2048,256]{2,1,0:T(8,128)(2,1)} fusion(bf16[512,2048]{1,0:T(8,128)(2,1)S(1)} %bitcast.210, bf16[512,256]{1,0:T(8,128)(2,1)S(1)} %get-tuple-element.62), kind=kOutput, calls=%fused_computation.5 | convolution fusion | flops 537395200 | bytes 3407872 | tf_op jit(solution)/shard_map/dot_general | solution.py:454
  72.4 1.7 %fusion = bf16[1,2048,256]{2,1,0:T(8,128)(2,1)} fusion(bf16[512,2048]{1,0:T(8,128)(2,1)S(1)} %bitcast.211, bf16[512,256]{1,0:T(8,128)(2,1)S(1)} %get-tuple-element.63), kind=kOutput, calls=%fused_computation.4 | convolution fusion | flops 537395200 | bytes 3407872 | tf_op jit(solution)/shard_map/dot_general | solution.py:454
  74.1 0.7 fusion.24
  74.9 0.5 copy-done.4
  75.3 2.1 %add_convert_fusion = bf16[512,2048]{1,0:T(8,128)(2,1)} fusion(f32[512,2048]{1,0:T(8,128)S(1)} %fusion.24, bf16[512,256]{1,0:T(8,128)(2,1)S(1)} %get-tuple-element.62, bf16[1,2048,256]{2,1,0:T(8,128)(2,1)S(1)} %copy-done.4), kind=kOutput, calls=%fused_computation | convolution fusion | flops 538968064 | bytes 7602176 | tf_op jit(solution)/shard_map/dot_general | solution.py:454
  77.4 47.4 %give_back.1 = (bf16[128,2048]{1,0:T(8,128)(2,1)}, bf16[8,128,512]{2,1,0:T(8,128)(2,1)}) custom-call(bf16[8,64,2048]{2,1,0:T(8,128)(2,1)} %bitcast.194, bf16[128,512]{1,0:T(8,128)(2,1)} %fusion.38.comb, bf16[128,512]{1,0:T(8,128)(2,1)} %copy-done.5, bf16[128,512]{1,0:T(8,128)(2,1)} %bitcast.201), custom_call_target="tpu_custom_call" | custom-call | tf_op jit(solution)/shard_map/give_back/pallas_call | solution.py:347
  124.9 2.9 %fusion.93 = f32[128,512]{0,1:T(8,128)} fusion(bf16[128,2048]{1,0:T(8,128)(2,1)} %get-tuple-element.19.resid, bf16[2048,512]{1,0:T(8,128)(2,1)S(1)} %copy-done), kind=kOutput, calls=%fused_computation.166 | convolution fusion | flops 268435456 | bytes 2883584 | tf_op jit(solution)/shard_map/dot_general | solution.py:575
  127.7 1.1 copy.218
  128.8 0.9 fusion.28
  129.7 0.8 fusion.29
  130.5 0.4 fusion.94
  130.9 1.0 fusion.18
  132.0 0.2 fusion.73
  132.1 0.2 fusion.61
  132.4 0.8 convolution_convert_fusion.4.state
  133.2 0.2 convolution_bitcast_fusion.2
  133.7 1.0 fusion.16
  134.6 0.7 copy.238
  135.3 30.3 %swap.1 = (bf16[8,128,256]{2,1,0:T(8,128)(2,1)}, bf16[8,2,128,256]{3,2,1,0:T(8,128)(2,1)}) custom-call(bf16[128,2048]{1,0:T(8,128)(2,1)} %get-tuple-element.19.resid, bf16[2,128,256]{2,1,0:T(8,128)(2,1)} %convolution_convert_fusion.4.state), custom_call_target="tpu_custom_call" | custom-call | tf_op jit(solution)/shard_map/swap/pallas_call | solution.py:405
  165.7 2.7 %convolution_bitcast_fusion = f32[256,512]{1,0:T(8,128)} fusion(bf16[8,128,256]{2,1,0:T(8,128)(2,1)} %get-tuple-element.20, bf16[8,128,512]{2,1,0:T(8,128)(2,1)} %get-tuple-element.21), kind=kOutput, calls=%fused_computation.12 | convolution fusion | flops 268435456 | bytes 2097152 | tf_op jit(solution)/shard_map/dot_general | solution.py:454
  168.5 0.3 multiply_reduce_fusion
  168.8 0.2 fusion.6
  169.1 0.2 fusion.49
  169.3 0.3 fusion.17
  169.6 0.7 copy.239
  170.3 0.8 copy.240
  (75 shorter events, 1.6 us)
Async XLA Ops:
  0.6 124.2 %copy-start = (bf16[2048,512]{1,0:T(8,128)(2,1)S(1)}, bf16[2048,512]{1,0:T(8,128)(2,1)}, u32[]{:S(2)}) copy-start(bf16[2048,512]{1,0:T(8,128)(2,1)} %param.20) | copy-start | bytes 6291460
  0.6 11.8 %copy-start.1 = (bf16[128,2,256]{2,1,0:T(2,128)(2,1)S(1)}, bf16[128,2,256]{2,1,0:T(2,128)(2,1)}, u32[]{:S(2)}) copy-start(bf16[128,2,256]{2,1,0:T(2,128)(2,1)} %param.18) | copy-start | bytes 393220
  0.8 57.7 %copy-start.21 = (pred[8]{0:T(512)(128)(4,1)}, pred[8]{0:T(512)(128)(4,1)S(1)}, u32[]{:S(2)}) copy-start(pred[8]{0:T(512)(128)(4,1)S(1)} %get-tuple-element.81) | copy-start | bytes 28
  1.6 13.2 %copy-start.12 = (pred[128]{0:T(512)(128)(4,1)}, pred[128]{0:T(512)(128)(4,1)S(1)}, u32[]{:S(2)}) copy-start(pred[128]{0:T(512)(128)(4,1)S(1)} %get-tuple-element.79) | copy-start | bytes 388
  1.6 13.2 %copy-start.14 = (pred[128]{0:T(512)(128)(4,1)}, pred[128]{0:T(512)(128)(4,1)S(1)}, u32[]{:S(2)}) copy-start(pred[128]{0:T(512)(128)(4,1)S(1)} %get-tuple-element.80) | copy-start | bytes 388
  1.6 13.2 %copy-start.16 = (s32[128]{0:T(128)}, s32[128]{0:T(128)S(1)}, u32[]{:S(2)}) copy-start(s32[128]{0:T(128)S(1)} %get-tuple-element.83) | copy-start | bytes 1540
  1.7 13.1 %copy-start.18 = (s32[128]{0:T(128)}, s32[128]{0:T(128)S(1)}, u32[]{:S(2)}) copy-start(s32[128]{0:T(128)S(1)} %get-tuple-element.84) | copy-start | bytes 1540
  7.1 9.7 %copy-start.6 = (f32[128,2]{0,1:T(2,128)}, f32[128,2]{0,1:T(2,128)S(1)}, u32[]{:S(2)}) copy-start(f32[128,2]{0,1:T(2,128)S(1)} %copy.201) | copy-start | bytes 3076
  8.0 60.9 %copy-start.8 = (f32[2,128]{1,0:T(2,128)}, f32[2,128]{1,0:T(2,128)S(1)}, u32[]{:S(2)}) copy-start(f32[2,128]{1,0:T(2,128)S(1)} %get-tuple-element.73) | copy-start | bytes 3076
  9.3 60.5 %copy-start.11 = (f32[128,2]{0,1:T(2,128)}, f32[128,2]{0,1:T(2,128)S(1)}, u32[]{:S(2)}) copy-start(f32[128,2]{0,1:T(2,128)S(1)} %copy.212) | copy-start | bytes 3076
  11.3 46.1 %copy-start.5 = (bf16[128,512]{1,0:T(8,128)(2,1)}, bf16[128,512]{1,0:T(8,128)(2,1)S(1)}, u32[]{:S(2)}) copy-start(bf16[128,512]{1,0:T(8,128)(2,1)S(1)} %constant_dynamic-slice_fusion.og) | copy-start | bytes 393220
  60.9 3.3 %copy-start.3 = (bf16[1,2048,256]{2,1,0:T(8,128)(2,1)S(1)}, bf16[1,2048,256]{2,1,0:T(8,128)(2,1)}, u32[]{:S(2)}) copy-start(bf16[1,2048,256]{2,1,0:T(8,128)(2,1)} %param.21) | copy-start | bytes 3145732
  60.9 3.3 %copy-start.23 = (bf16[8,64,2048]{2,1,0:T(8,128)(2,1)S(1)}, bf16[8,64,2048]{2,1,0:T(8,128)(2,1)}, u32[]{:S(2)}) copy-start(bf16[8,64,2048]{2,1,0:T(8,128)(2,1)} %get-tuple-element.15) | copy-start | bytes 6291460
  64.2 1.6 copy-start.24
  64.2 1.8 %copy-start.25 = (bf16[1,256,2048]{2,1,0:T(8,128)(2,1)S(1)}, bf16[1,256,2048]{2,1,0:T(8,128)(2,1)}, u32[]{:S(2)}) copy-start(bf16[1,256,2048]{2,1,0:T(8,128)(2,1)} %param.23) | copy-start | bytes 3145732
  74.1 1.2 copy-start.4
  128.8 3.5 %copy-start.9 = (f32[2,128]{1,0:T(2,128)S(1)}, f32[2,128]{1,0:T(2,128)}, u32[]{:S(2)}) copy-start(f32[2,128]{1,0:T(2,128)} %copy-done.8) | copy-start | bytes 3076
  133.4 35.0 %copy-start.7 = (f32[8,2]{1,0:T(8,128)S(1)}, f32[8,2]{1,0:T(8,128)}, u32[]{:S(2)}) copy-start(f32[8,2]{1,0:T(8,128)} %copy.231) | copy-start | bytes 196
  133.4 35.0 %copy-start.22 = (pred[8]{0:T(512)(128)(4,1)S(1)}, pred[8]{0:T(512)(128)(4,1)}, u32[]{:S(2)}) copy-start(pred[8]{0:T(512)(128)(4,1)} %copy-done.21) | copy-start | bytes 28
  134.6 34.2 %copy-start.10 = (f32[128,2]{0,1:T(2,128)S(1)}, f32[128,2]{0,1:T(2,128)}, u32[]{:S(2)}) copy-start(f32[128,2]{0,1:T(2,128)} %copy.230) | copy-start | bytes 3076
  165.7 2.8 %copy-start.2 = (bf16[8,2,128,256]{3,2,1,0:T(8,128)(2,1)S(1)}, bf16[8,2,128,256]{3,2,1,0:T(8,128)(2,1)}, u32[]{:S(2)}) copy-start(bf16[8,2,128,256]{3,2,1,0:T(8,128)(2,1)} %get-tuple-element.22) | copy-start | bytes 3145732
  165.7 3.6 %copy-start.13 = (pred[128]{0:T(512)(128)(4,1)S(1)}, pred[128]{0:T(512)(128)(4,1)}, u32[]{:S(2)}) copy-start(pred[128]{0:T(512)(128)(4,1)} %copy-done.12) | copy-start | bytes 388
  165.7 3.6 %copy-start.15 = (pred[128]{0:T(512)(128)(4,1)S(1)}, pred[128]{0:T(512)(128)(4,1)}, u32[]{:S(2)}) copy-start(pred[128]{0:T(512)(128)(4,1)} %copy-done.14) | copy-start | bytes 388
  165.7 3.6 %copy-start.17 = (s32[128]{0:T(128)S(1)}, s32[128]{0:T(128)}, u32[]{:S(2)}) copy-start(s32[128]{0:T(128)} %copy-done.16) | copy-start | bytes 1540
  165.7 3.6 %copy-start.19 = (s32[128]{0:T(128)S(1)}, s32[128]{0:T(128)}, u32[]{:S(2)}) copy-start(s32[128]{0:T(128)} %copy-done.18) | copy-start | bytes 1540
  165.7 3.6 %copy-start.20 = (f32[2,128]{1,0:T(2,128)S(1)}, f32[2,128]{1,0:T(2,128)}, u32[]{:S(2)}) copy-start(f32[2,128]{1,0:T(2,128)} %get-tuple-element.61) | copy-start | bytes 3076

commit v3 on v2

--- a/solution.py
+++ b/solution.py
@@ -308,8 +308,10 @@
             second(order[n - lag])
         if n >= lag + 1 and order[n - lag - 1] != 0:
             to_home(order[n - lag - 1])
-        if n and n % 2 == 0 and n < n_sp:
-            chain.step(n // 2)
+        if n and n % 3 == 0 and n // 3 < n_sp // 2:
+            chain.step(n // 3)
+    for d in range((n_sp + lag) // 3 + 1, n_sp // 2):
+        chain.step(d)
     for k in range(1, n_sp):
         source = lax.rem(me + n_sp - k, n_sp)
         push(sendbuf.at[k], ret.at[source], ssem.at[k], rsem.at[k], (me, far)).wait_recv()
@@ -364,7 +366,10 @@
     )(back, comb, og_q, normed)
 
 
-def swap_kernel(n_sp, w, resid, state, cols_out, states, own_sem, ssem, rsem, *chain_sem):
+def swap_kernel(
+    n_sp, w, tile, resid, state, rows, grads, act, gate_back, up_back,
+    cols_out, states, gate_out, up_out, down_out, own_sem, ssem, rsem, *chain_sem,
+):
     me = lax.axis_index("sp")
     c = lax.axis_index("tp")
     greet(n_sp, me, c, True, ())
@@ -377,15 +382,34 @@
     chain = Chain(state, states, n_sp, me, c, chain_sem, (1,))
     chain.start()
     waits = []
-    for k in range(1, n_sp):
-        peer = lax.rem(me + k, n_sp)
-        cp = push(part(peer), cols_out.at[me], ssem.at[k], rsem.at[k], (peer, c))
+
+    def send(k):
+        cp = push(
+            part(lax.rem(me + k, n_sp)), cols_out.at[me], ssem.at[k], rsem.at[k],
+            (lax.rem(me + k, n_sp), c),
+        )
         cp.start()
         waits.append(cp)
+
     local = pltpu.make_async_copy(part(me), cols_out.at[me], own_sem.at[0])
     local.start()
-    for d in range(1, n_sp // 2):
+    tiles = rows.shape[1] // tile
+
+    def outer(lo, hi):
+        @pl.loop(lo, hi)
+        def _(i):
+            span = pl.ds(pl.multiple_of(i * tile, tile), tile)
+            gate_out[span, :] = mm(rows[:, span], gate_back[...], 0, 0).astype(BF16)
+            up_out[span, :] = mm(rows[:, span], up_back[...], 0, 0).astype(BF16)
+            down_out[:, span] = mm(act[...], grads[:, span], 0, 0).astype(BF16)
+
+    steps = n_sp // 2
+    for d in range(1, steps):
+        send(2 * d)
+        send(2 * d - 1)
+        outer(tiles * (d - 1) // (steps - 1), tiles * d // (steps - 1))
         chain.step(d)
+    send(n_sp - 1)
     for k in range(1, n_sp):
         source = lax.rem(me + n_sp - k, n_sp)
         spot = cols_out.at[source]
@@ -396,24 +420,29 @@
     chain.finish()
 
 
-def swap(resid, state, n_sp):
+def swap(resid, state, rows, grads, act, gate_back, up_back, n_sp):
     tokens, width = resid.shape
     w = width // n_sp
     if w % 128:
         resid = resid.reshape(tokens, n_sp, w).transpose(1, 0, 2)
+    hidden = act.shape[1]
+    tile = width // 8
     dma = pltpu.SemaphoreType.DMA
     return pl.pallas_call(
-        functools.partial(swap_kernel, n_sp, w),
+        functools.partial(swap_kernel, n_sp, w, tile),
         out_shape=(
             jax.ShapeDtypeStruct((n_sp, tokens, w), BF16),
             jax.ShapeDtypeStruct((n_sp,) + state.shape, BF16),
+            jax.ShapeDtypeStruct((width, hidden), BF16),
+            jax.ShapeDtypeStruct((width, hidden), BF16),
+            jax.ShapeDtypeStruct((hidden, width), BF16),
         ),
-        in_specs=any_specs(2),
-        out_specs=tuple(any_specs(2)),
+        in_specs=any_specs(2) + vmem_specs(5),
+        out_specs=tuple(any_specs(2) + vmem_specs(3)),
         scratch_shapes=[dma((1,)), dma((n_sp,)), dma((n_sp,))] + chain_sems(n_sp),
         compiler_params=pltpu.CompilerParams(collective_id=2, has_side_effects=True),
         name="swap",
-    )(resid, state)
+    )(resid, state, rows, grads, act, gate_back, up_back)
 
 
 def rotation_tables(start, count, key_width):
@@ -461,7 +490,6 @@
     up_clip = jnp.clip(up_pre, -CLAMP_LIMIT, CLAMP_LIMIT)
     sigmoid_gate = jax.nn.sigmoid(GATE_SLOPE * gate_clip)
     activated = (gate_clip * sigmoid_gate * (up_clip + 1.0)).astype(BF16)
-    down_part = mm(activated, routed_grads, 0, 0)
     act_grad = mm(routed_grads, down_w, 1, 1)
     slope = sigmoid_gate + GATE_SLOPE * gate_clip * sigmoid_gate * (1.0 - sigmoid_gate)
     gate_pre_grad = jnp.where(
@@ -470,15 +498,8 @@
     up_pre_grad = jnp.where(
         jnp.abs(up_pre) < CLAMP_LIMIT, act_grad * gate_clip * sigmoid_gate, 0.0
     ).astype(BF16)
-    gate_part = mm(routed_rows, gate_pre_grad, 0, 0)
-    up_part = mm(routed_rows, up_pre_grad, 0, 0)
     back_rows = mm(gate_pre_grad, gate_w, 1, 1) + mm(up_pre_grad, up_w, 1, 1)
-    return (
-        gate_part.astype(BF16),
-        up_part.astype(BF16),
-        down_part.astype(BF16),
-        back_rows.astype(BF16),
-    )
+    return activated, gate_pre_grad, up_pre_grad, back_rows.astype(BF16)
 
 
 def per_device(
@@ -548,7 +569,7 @@
     weights = fine("hik,hjk->hij", query_rot, key_rot) * mask
     retained_local = fine("hij,hjv->hiv", weights, values)
 
-    gate_part, up_part, down_part, back_rows = expert_local(
+    activated, gate_back, up_back, back_rows = expert_local(
         rows.reshape(slots, width),
         grads.reshape(slots, width),
         gate_weight[0],
@@ -579,7 +600,16 @@
     )
     grad_bf = grad.astype(BF16)
     inner_grad = ein("gwn,gwj->gnj", query_rot * decay, grad_bf).astype(BF16)
-    resid_cols, grads_all = swap(resid, inner_grad, n_sp)
+    resid_cols, grads_all, gate_part, up_part, down_part = swap(
+        resid,
+        inner_grad,
+        rows.reshape(slots, width),
+        grads.reshape(slots, width),
+        activated,
+        gate_back,
+        up_back,
+        n_sp,
+    )
     future = weighted(grads_all, coming, ids > me).astype(BF16)
     score = fine("hiv,hjv->hij", grad, values) * mask
     query_portion = ein("hij,hjk->hik", score, key_bf) + decay * fine(

time: 172 us -> 178 us (1.035)
  other arithmetic: 9.13 us -> 13.7 us
  local copies, waits for them, and re-layouts: 13.9 us -> 16.6 us
    pallas_call x1, Pallas kernels: 47.4 us -> 41.4 us  [give_back(): pl.pallas_call(functools.partial(return_kernel, n_sp, n_tp, q), out_shape...]
    pallas_call x1, Pallas kernels: 30.3 us -> 35.3 us  [swap(): pl.pallas_call(functools.partial(swap_kernel, n_sp, w, tile), out_shape=(...]
    dot_general x9 -> x6, matrix products: 15.3 us -> 10.9 us  [mm(): lax.dot_general(a, b, (((da,), (db,)), ((), ())), preferred_element_type=...]
    dot_general x7, matrix products: 2.69 us -> 6.7 us  [ein(): jnp.einsum(spec, a.astype(BF16), b.astype(BF16), preferred_element_type=F32)]
    unnamed x58 -> x85, local copies, waits for them, and re-layouts: 6.61 us -> 9.55 us
where the time goes in v3:
time: 178 us; the launch traced here: 177 us
  Pallas kernels  117 us (66%)
  matrix products  28.2 us (16%)
  local copies, waits for them, and re-layouts  16.6 us (9%)
  other arithmetic  13.7 us (8%)
    pallas_call x1, Pallas kernels, give_back(): pl.pallas_call(functools.partial(return_kernel, n_sp, n_tp, q), out_shape...  41.4 us
    pallas_call x1, Pallas kernels, dispatch(): pl.pallas_call(functools.partial(dispatch_kernel, n_sp, n_tp, q), out_sha...  40.5 us
    pallas_call x1, Pallas kernels, swap(): pl.pallas_call(functools.partial(swap_kernel, n_sp, w, tile), out_shape=(...  35.3 us
    dot_general x6, matrix products, mm(): lax.dot_general(a, b, (((da,), (db,)), ((), ())), preferred_element_type=...  10.9 us
    unnamed x85, local copies, waits for them, and re-layouts  9.55 us
    dot_general x7, matrix products, ein(): jnp.einsum(spec, a.astype(BF16), b.astype(BF16), preferred_element_type=F32)  6.7 us

profile of v3, /device:TPU:0, one launch (start us, length us, event | category | flops | bytes accessed | tf_op | source)
XLA Modules:
  0.0 176.9 jit_solution(5499816847985263906)
XLA Ops:
  1.0 1.0 fusion.71
  2.0 1.0 copy.202
  3.0 0.3 fusion.5
  3.3 0.8 copy.200
  4.1 0.2 reduce_window_sum.22
  4.3 0.2 slice_reduce_fusion
  4.5 0.7 broadcast_multiply_fusion.1
  5.2 1.7 convolution_convert_fusion.2.state
  6.9 0.9 constant_dynamic-slice_fusion.og
  7.8 0.7 convert_reduce_fusion
  8.7 0.7 select_reduce_fusion
  9.4 0.7 convert_add_fusion
  10.2 0.8 slice_bitcast_fusion.5
  11.1 1.1 fusion
  12.2 2.0 %convolution_convert_fusion = bf16[512,512]{1,0:T(8,128)(2,1)} fusion(bf16[128,2048]{1,0:T(8,128)(2,1)} %param.12, s32[]{:T(128)S(6)} %select_n.92, pred[2,512,128]{2,1,0:T(32,128)(4,1)S(1)} %iota_compare_fusion), kind=kOutput, calls=%fused_computation.5 | convolution fusion | flops 67436544 | bytes 786436 | tf_op jit(solution)/shard_map/dot_general | solution.py:540
  14.2 0.6 broadcast_in_dim.167.tot
  14.8 40.5 %dispatch.1 = (bf16[8,64,2048]{2,1,0:T(8,128)(2,1)}, bf16[8,64,2048]{2,1,0:T(8,128)(2,1)}, f32[8,8,128]{2,1,0:T(8,128)}, bf16[8,2,128,256]{3,2,1,0:T(8,128)(2,1)}) custom-call(bf16[8,64,512]{2,1,0:T(8,128)(2,1)} %bitcast.187, bf16[8,64,512]{2,1,0:T(8,128)(2,1)} %bitcast.202, f32[8,128]{1,0:T(8,128)} %broadcast_in_dim.167.tot, ...), custom_call_target="tpu_custom_call" | custom-call | tf_op jit(solution)/shard_map/dispatch/pallas_call | solution.py:228
  55.3 0.8 slice.33
  56.3 0.2 reduce_window_sum.23
  56.5 0.6 exponential_select_fusion.1
  57.2 1.6 multiply_reduce_fusion.1
  59.0 0.3 fusion.7
  59.3 0.4 fusion.81
  59.8 0.4 convolution_multiply_fusion.2
  60.2 0.7 copy-done.4
  60.8 1.0 multiply_reduce_fusion.2
  61.8 0.6 add_rsqrt_fusion
  62.4 1.5 subtract_exponential_fusion
  63.9 1.4 copy.212
  65.4 0.8 fusion.33
  66.2 0.6 copy.263
  66.8 2.9 %fusion.17 = f32[512,256]{1,0:T(8,128)S(1)} fusion(bf16[512,2048]{1,0:T(8,128)(2,1)} %bitcast.192, bf16[1,2048,256]{2,1,0:T(8,128)(2,1)} %param.22), kind=kOutput, calls=%fused_computation.33 | convolution fusion | flops 536870912 | bytes 3670016 | tf_op jit(solution)/shard_map/dot_general | solution.py:483
  69.8 0.7 fusion.23
  70.5 0.8 copy-done.3
  71.4 0.3 copy-done.37
  71.6 1.7 select_convert_fusion
  73.4 0.7 fusion.21
  74.1 0.6 copy-done.12
  74.8 2.1 %add_convert_fusion = bf16[512,2048]{1,0:T(8,128)(2,1)} fusion(f32[512,2048]{1,0:T(8,128)S(1)} %fusion.21, bf16[512,256]{1,0:T(8,128)(2,1)S(1)} %get-tuple-element.68.up_back, bf16[1,2048,256]{2,1,0:T(8,128)(2,1)S(1)} %copy-done.12), kind=kOutput, calls=%fused_computation | convolution fusion | flops 538968064 | bytes 7602176 | tf_op jit(solution)/shard_map/dot_general | solution.py:483
  76.9 0.8 fusion.31.comb
  77.6 41.4 %give_back.1 = (bf16[128,2048]{1,0:T(8,128)(2,1)}, bf16[8,128,512]{2,1,0:T(8,128)(2,1)}) custom-call(bf16[8,64,2048]{2,1,0:T(8,128)(2,1)} %bitcast.186, bf16[128,512]{1,0:T(8,128)(2,1)} %fusion.31.comb, bf16[128,512]{1,0:T(8,128)(2,1)} %copy-done.19, bf16[128,512]{1,0:T(8,128)(2,1)} %bitcast.201), custom_call_target="tpu_custom_call" | custom-call | tf_op jit(solution)/shard_map/give_back/pallas_call | solution.py:349
  119.0 2.0 %fusion.82 = f32[128,512]{0,1:T(8,128)S(1)} fusion(bf16[128,2048]{1,0:T(8,128)(2,1)} %get-tuple-element.22.resid, bf16[2048,512]{1,0:T(8,128)(2,1)S(1)} %copy-done), kind=kOutput, calls=%fused_computation.152 | convolution fusion | flops 268435456 | bytes 2883584 | tf_op jit(solution)/shard_map/dot_general | solution.py:596
  121.2 0.9 fusion.25
  122.0 0.8 fusion.26
  122.8 1.4 convolution_convert_fusion.1.state
  124.3 35.3 %swap.1 = (bf16[8,128,256]{2,1,0:T(8,128)(2,1)}, bf16[8,2,128,256]{3,2,1,0:T(8,128)(2,1)}, bf16[2048,256]{1,0:T(8,128)(2,1)}, bf16[2048,256]{1,0:T(8,128)(2,1)}, bf16[256,2048]{1,0:T(8,128)(2,1)}) custom-call(bf16[128,2048]{1,0:T(8,128)(2,1)} %get-tuple-element.22.resid, bf16[2,128,256]{2,1,0:T(8,128)(2,1)} %convolution_convert_fusion.1.state, ...), custom_call_target="tpu_custom_call" | custom-call | tf_op jit(solution)/shard_map/swap/pallas_call | solution.py:431
  159.8 1.6 multiply_reduce_fusion
  161.4 0.9 convolution_bitcast_fusion.2
  162.4 1.2 fusion.3
  163.6 0.8 copy.240
  164.4 0.2 fusion.42
  164.6 0.3 fusion.15
  164.9 0.2 fusion.54
  165.3 1.0 fusion.14
  166.4 0.7 copy.239
  167.1 0.4 fusion.83
  167.5 0.8 copy.224
  168.2 1.0 fusion.66
  169.3 1.2 fusion.13
  170.6 0.7 copy.238
  171.3 2.7 %convolution_bitcast_fusion = f32[256,512]{1,0:T(8,128)} fusion(bf16[8,128,256]{2,1,0:T(8,128)(2,1)} %get-tuple-element.26, bf16[8,128,512]{2,1,0:T(8,128)(2,1)} %get-tuple-element.27), kind=kOutput, calls=%fused_computation.6 | convolution fusion | flops 268435456 | bytes 2097152 | tf_op jit(solution)/shard_map/dot_general | solution.py:483
  174.0 1.0 copy.278
  175.0 1.0 copy.279
  176.0 1.0 copy.280
  (99 shorter events, 1.9 us)
Async XLA Ops:
  0.6 118.4 %copy-start = (bf16[2048,512]{1,0:T(8,128)(2,1)S(1)}, bf16[2048,512]{1,0:T(8,128)(2,1)}, u32[]{:S(2)}) copy-start(bf16[2048,512]{1,0:T(8,128)(2,1)} %param.20) | copy-start | bytes 6291460
  1.9 57.0 %copy-start.6 = (f32[128,128]{0,1:T(8,128)}, f32[128,128]{0,1:T(8,128)S(1)}, u32[]{:S(2)}) copy-start(f32[128,128]{0,1:T(8,128)S(1)} %get-tuple-element.77) | copy-start | bytes 196612
  1.9 57.0 %copy-start.28 = (pred[128]{0:T(512)(128)(4,1)}, pred[128]{0:T(512)(128)(4,1)S(1)}, u32[]{:S(2)}) copy-start(pred[128]{0:T(512)(128)(4,1)S(1)} %get-tuple-element.86) | copy-start | bytes 388
  1.9 57.0 %copy-start.29 = (pred[128]{0:T(512)(128)(4,1)}, pred[128]{0:T(512)(128)(4,1)S(1)}, u32[]{:S(2)}) copy-start(pred[128]{0:T(512)(128)(4,1)S(1)} %get-tuple-element.87) | copy-start | bytes 388
  2.0 57.0 %copy-start.30 = (s32[128]{0:T(128)}, s32[128]{0:T(128)S(1)}, u32[]{:S(2)}) copy-start(s32[128]{0:T(128)S(1)} %get-tuple-element.90) | copy-start | bytes 1540
  2.0 57.0 %copy-start.31 = (s32[128]{0:T(128)}, s32[128]{0:T(128)S(1)}, u32[]{:S(2)}) copy-start(s32[128]{0:T(128)S(1)} %get-tuple-element.91) | copy-start | bytes 1540
  4.2 5.8 %copy-start.15 = (f32[128,2]{1,0:T(8,128)}, f32[128,2]{1,0:T(8,128)S(1)}, u32[]{:S(2)}) copy-start(f32[128,2]{1,0:T(8,128)S(1)} %reduce_window_sum.22) | copy-start | bytes 3076
  4.3 55.5 %copy-start.23 = (f32[128,2]{0,1:T(2,128)}, f32[128,2]{0,1:T(2,128)S(1)}, u32[]{:S(2)}) copy-start(f32[128,2]{0,1:T(2,128)S(1)} %copy.201) | copy-start | bytes 3076
  4.5 52.0 %copy-start.35 = (f32[2]{0:T(128)}, f32[2]{0:T(128)S(1)}, u32[]{:S(2)}) copy-start(f32[2]{0:T(128)S(1)} %slice_reduce_fusion) | copy-start | bytes 28
  7.8 49.4 %copy-start.19 = (bf16[128,512]{1,0:T(8,128)(2,1)}, bf16[128,512]{1,0:T(8,128)(2,1)S(1)}, u32[]{:S(2)}) copy-start(bf16[128,512]{1,0:T(8,128)(2,1)S(1)} %constant_dynamic-slice_fusion.og) | copy-start | bytes 393220
  10.1 47.1 %copy-start.26 = (s32[128,2]{0,1:T(2,128)}, s32[128,2]{0,1:T(2,128)S(1)}, u32[]{:S(2)}) copy-start(s32[128,2]{0,1:T(2,128)S(1)} %convert_add_fusion) | copy-start | bytes 3076
  10.2 48.6 %copy-start.22 = (bf16[128,2,128]{2,1,0:T(2,128)(2,1)S(1)}, bf16[128,2,128]{2,1,0:T(2,128)(2,1)}, u32[]{:S(2)}) copy-start(bf16[128,2,128]{2,1,0:T(2,128)(2,1)} %param.16) | copy-start | bytes 196612
  14.2 46.6 %copy-start.1 = (bf16[128,2,256]{2,1,0:T(2,128)(2,1)S(1)}, bf16[128,2,256]{2,1,0:T(2,128)(2,1)}, u32[]{:S(2)}) copy-start(bf16[128,2,256]{2,1,0:T(2,128)(2,1)} %param.18) | copy-start | bytes 393220
  56.2 2.6 %copy-start.33 = (pred[8]{0:T(512)(128)(4,1)}, pred[8]{0:T(512)(128)(4,1)S(1)}, u32[]{:S(2)}) copy-start(pred[8]{0:T(512)(128)(4,1)S(1)} %get-tuple-element.88) | copy-start | bytes 28
  59.0 3.4 %copy-start.36 = (f32[2]{0:T(128)S(1)}, f32[2]{0:T(128)}, u32[]{:S(2)}) copy-start(f32[2]{0:T(128)} %copy-done.35) | copy-start | bytes 28
  60.2 0.7 copy-start.4
  66.2 3.6 %copy-start.2 = (bf16[8,64,2048]{2,1,0:T(8,128)(2,1)S(1)}, bf16[8,64,2048]{2,1,0:T(8,128)(2,1)}, u32[]{:S(2)}) copy-start(bf16[8,64,2048]{2,1,0:T(8,128)(2,1)} %get-tuple-element.18) | copy-start | bytes 6291460
  66.2 3.6 %copy-start.11 = (bf16[1,2048,256]{2,1,0:T(8,128)(2,1)S(1)}, bf16[1,2048,256]{2,1,0:T(8,128)(2,1)}, u32[]{:S(2)}) copy-start(bf16[1,2048,256]{2,1,0:T(8,128)(2,1)} %param.21) | copy-start | bytes 3145732
  69.8 1.6 copy-start.3
  69.8 1.8 %copy-start.37 = (bf16[1,256,2048]{2,1,0:T(8,128)(2,1)S(1)}, bf16[1,256,2048]{2,1,0:T(8,128)(2,1)}, u32[]{:S(2)}) copy-start(bf16[1,256,2048]{2,1,0:T(8,128)(2,1)} %param.23) | copy-start | bytes 3145732
  73.4 0.8 copy-start.13
  73.4 0.8 copy-start.14
  73.4 1.4 copy-start.12
  74.8 2.1 %copy-start.27 = (s32[128,2]{0,1:T(2,128)S(1)}, s32[128,2]{0,1:T(2,128)}, u32[]{:S(2)}) copy-start(s32[128,2]{0,1:T(2,128)} %copy-done.26) | copy-start | bytes 3076
  124.3 35.4 %copy-start.32 = (f32[8,2]{0,1:T(2,128)S(1)}, f32[8,2]{0,1:T(2,128)}, u32[]{:S(2)}) copy-start(f32[8,2]{0,1:T(2,128)} %get-tuple-element.73) | copy-start | bytes 196
  124.3 35.5 %copy-start.34 = (pred[8]{0:T(512)(128)(4,1)S(1)}, pred[8]{0:T(512)(128)(4,1)}, u32[]{:S(2)}) copy-start(pred[8]{0:T(512)(128)(4,1)} %copy-done.33) | copy-start | bytes 28
  124.3 37.1 %copy-start.5 = (f32[2,128,128]{2,1,0:T(8,128)S(1)}, f32[2,128,128]{2,1,0:T(8,128)}, u32[]{:S(2)}) copy-start(f32[2,128,128]{2,1,0:T(8,128)} %copy-done.4) | copy-start | bytes 393220
  124.3 38.0 %copy-start.21 = (f32[128,2]{1,0:T(8,128)S(1)}, f32[128,2]{1,0:T(8,128)}, u32[]{:S(2)}) copy-start(f32[128,2]{1,0:T(8,128)} %get-tuple-element.71) | copy-start | bytes 3076
  159.7 4.9 %copy-start.24 = (f32[128,2]{0,1:T(2,128)S(1)}, f32[128,2]{0,1:T(2,128)}, u32[]{:S(2)}) copy-start(f32[128,2]{0,1:T(2,128)} %copy-done.23) | copy-start | bytes 3076
  159.7 5.4 %copy-start.7 = (f32[128,128]{0,1:T(8,128)S(1)}, f32[128,128]{0,1:T(8,128)}, u32[]{:S(2)}) copy-start(f32[128,128]{0,1:T(8,128)} %copy-done.6) | copy-start | bytes 196612
  159.7 5.5 %copy-start.20 = (f32[128,128]{0,1:T(8,128)S(1)}, f32[128,128]{0,1:T(8,128)}, u32[]{:S(2)}) copy-start(f32[128,128]{0,1:T(8,128)} %get-tuple-element.75) | copy-start | bytes 196612
  162.4 2.2 %copy-start.25 = (f32[128,2]{0,1:T(2,128)}, f32[128,2]{0,1:T(2,128)S(1)}, u32[]{:S(2)}) copy-start(f32[128,2]{0,1:T(2,128)S(1)} %copy.230) | copy-start | bytes 3076
  164.8 2.2 %copy-start.16 = (bf16[2,128,128]{2,1,0:T(8,128)(2,1)}, bf16[2,128,128]{2,1,0:T(8,128)(2,1)S(1)}, u32[]{:S(2)}) copy-start(bf16[2,128,128]{2,1,0:T(8,128)(2,1)S(1)} %fusion.15) | copy-start | bytes 196612
  165.2 1.2 copy-start.17
  165.3 1.1 copy-start.18
  167.5 6.6 %copy-start.10 = (bf16[2048,256]{1,0:T(8,128)(2,1)S(1)}, bf16[2048,256]{1,0:T(8,128)(2,1)}, u32[]{:S(2)}) copy-start(bf16[2048,256]{1,0:T(8,128)(2,1)} %get-tuple-element.23) | copy-start | bytes 3145732
  171.3 3.7 %copy-start.9 = (bf16[2048,256]{1,0:T(8,128)(2,1)S(1)}, bf16[2048,256]{1,0:T(8,128)(2,1)}, u32[]{:S(2)}) copy-start(bf16[2048,256]{1,0:T(8,128)(2,1)} %get-tuple-element.24) | copy-start | bytes 3145732
  174.0 1.9 %copy-start.8 = (bf16[256,2048]{1,0:T(8,128)(2,1)S(1)}, bf16[256,2048]{1,0:T(8,128)(2,1)}, u32[]{:S(2)}) copy-start(bf16[256,2048]{1,0:T(8,128)(2,1)} %get-tuple-element.25) | copy-start | bytes 3145732

commit v4 on v2

--- a/solution.py
+++ b/solution.py
@@ -308,8 +308,10 @@
             second(order[n - lag])
         if n >= lag + 1 and order[n - lag - 1] != 0:
             to_home(order[n - lag - 1])
-        if n and n % 2 == 0 and n < n_sp:
-            chain.step(n // 2)
+        if n and n % 3 == 0 and n // 3 < n_sp // 2:
+            chain.step(n // 3)
+    for d in range((n_sp + lag) // 3 + 1, n_sp // 2):
+        chain.step(d)
     for k in range(1, n_sp):
         source = lax.rem(me + n_sp - k, n_sp)
         push(sendbuf.at[k], ret.at[source], ssem.at[k], rsem.at[k], (me, far)).wait_recv()
@@ -377,15 +379,20 @@
     chain = Chain(state, states, n_sp, me, c, chain_sem, (1,))
     chain.start()
     waits = []
-    for k in range(1, n_sp):
+
+    def send(k):
         peer = lax.rem(me + k, n_sp)
         cp = push(part(peer), cols_out.at[me], ssem.at[k], rsem.at[k], (peer, c))
         cp.start()
         waits.append(cp)
+
     local = pltpu.make_async_copy(part(me), cols_out.at[me], own_sem.at[0])
     local.start()
     for d in range(1, n_sp // 2):
+        send(2 * d)
+        send(2 * d - 1)
         chain.step(d)
+    send(n_sp - 1)
     for k in range(1, n_sp):
         source = lax.rem(me + n_sp - k, n_sp)
         spot = cols_out.at[source]

time: 172 us -> 167 us (0.971)
  Pallas kernels: 118 us -> 113 us
    pallas_call x1, Pallas kernels: 47.4 us -> 41.3 us  [give_back(): pl.pallas_call(functools.partial(return_kernel, n_sp, n_tp, q), out_shape...]
where the time goes in v4:
time: 167 us; the launch traced here: 166 us
  Pallas kernels  113 us (68%)
  matrix products  28.6 us (17%)
  local copies, waits for them, and re-layouts  13.9 us (8%)
  other arithmetic  9.13 us (5%)
    pallas_call x1, Pallas kernels, give_back(): pl.pallas_call(functools.partial(return_kernel, n_sp, n_tp, q), out_shape...  41.3 us
    pallas_call x1, Pallas kernels, dispatch(): pl.pallas_call(functools.partial(dispatch_kernel, n_sp, n_tp, q), out_sha...  40.5 us
    pallas_call x1, Pallas kernels, swap(): pl.pallas_call(functools.partial(swap_kernel, n_sp, w), out_shape=(jax.Sh...  31.3 us
    dot_general x9, matrix products, mm(): lax.dot_general(a, b, (((da,), (db,)), ((), ())), preferred_element_type=...  15.3 us
    unnamed x58, local copies, waits for them, and re-layouts  6.61 us

profile of v4, /device:TPU:0, one launch (start us, length us, event | category | flops | bytes accessed | tf_op | source)
XLA Modules:
  0.0 165.9 jit_solution(13950932743710020655)
XLA Ops:
  0.8 0.8 slice_bitcast_fusion.5
  1.7 0.7 convert_reduce_fusion
  2.5 0.7 select_reduce_fusion
  3.2 0.7 convert_add_fusion
  4.0 0.1 mul.299
  4.1 1.0 copy.206
  5.1 1.0 copy.202
  6.1 0.8 copy.200
  6.9 0.2 reduce_window_sum.22
  7.1 0.2 slice_reduce_fusion
  7.3 0.7 broadcast_multiply_fusion.1
  8.0 0.6 broadcast_in_dim.167.tot
  8.6 0.7 copy.230
  9.3 0.8 fusion.38.comb
  10.2 0.2 add_reduce_fusion
  10.4 0.9 constant_dynamic-slice_fusion.og
  11.3 0.3 fusion.78
  11.7 0.3 fusion.10
  12.0 0.3 fusion.8
  12.5 0.8 convolution_convert_fusion.5.state
  13.3 0.4 convolution_multiply_fusion.2
  13.7 1.1 fusion.3
  14.8 2.0 %convolution_convert_fusion.3 = bf16[512,512]{1,0:T(8,128)(2,1)} fusion(bf16[128,2048]{1,0:T(8,128)(2,1)} %param.12, s32[]{:T(128)S(6)} %select_n.92, pred[2,512,128]{2,1,0:T(32,128)(4,1)S(1)} %iota_compare_fusion), kind=kOutput, calls=%fused_computation.11 | convolution fusion | flops 67436544 | bytes 786436 | tf_op jit(solution)/shard_map/dot_general | solution.py:526
  16.8 40.5 %dispatch.1 = (bf16[8,64,2048]{2,1,0:T(8,128)(2,1)}, bf16[8,64,2048]{2,1,0:T(8,128)(2,1)}, f32[8,8,128]{2,1,0:T(8,128)}, bf16[8,2,128,256]{3,2,1,0:T(8,128)(2,1)}) custom-call(bf16[8,64,512]{2,1,0:T(8,128)(2,1)} %bitcast.195, bf16[8,64,512]{2,1,0:T(8,128)(2,1)} %bitcast.202, f32[8,128]{1,0:T(8,128)} %broadcast_in_dim.167.tot, ...), custom_call_target="tpu_custom_call" | custom-call | tf_op jit(solution)/shard_map/dispatch/pallas_call | solution.py:228
  57.3 0.8 slice.33
  58.3 0.2 reduce_window_sum.23
  58.6 0.7 copy.231
  59.3 1.6 multiply_reduce_fusion.1
  61.0 0.4 fusion.92
  61.4 2.8 %fusion.20 = f32[512,256]{1,0:T(8,128)S(1)} fusion(bf16[512,2048]{1,0:T(8,128)(2,1)} %bitcast.208, bf16[1,2048,256]{2,1,0:T(8,128)(2,1)} %param.22), kind=kOutput, calls=%fused_computation.39 | convolution fusion | flops 536870912 | bytes 3670016 | tf_op jit(solution)/shard_map/dot_general | solution.py:461
  64.2 0.7 fusion.26
  65.0 0.9 copy-done.24
  65.8 0.3 copy-done.25
  66.1 1.0 select_convert_fusion
  67.1 1.8 %fusion.2 = bf16[1,256,2048]{2,1,0:T(8,128)(2,1)} fusion(bf16[512,2048]{1,0:T(8,128)(2,1)S(1)} %bitcast.213, f32[512,256]{1,0:T(8,128)S(1)} %fusion.26, f32[512,256]{1,0:T(8,128)S(1)} %fusion.20), kind=kOutput, calls=%fused_computation.6 | convolution fusion | flops 538705920 | bytes 4194304 | tf_op jit(solution)/shard_map/dot_general | solution.py:461
  68.9 0.3 multiply_reduce_fusion.2
  69.2 0.6 add_rsqrt_fusion
  70.0 0.7 copy.263
  70.6 1.8 %fusion.1 = bf16[1,2048,256]{2,1,0:T(8,128)(2,1)} fusion(bf16[512,2048]{1,0:T(8,128)(2,1)S(1)} %bitcast.210, bf16[512,256]{1,0:T(8,128)(2,1)S(1)} %get-tuple-element.62), kind=kOutput, calls=%fused_computation.5 | convolution fusion | flops 537395200 | bytes 3407872 | tf_op jit(solution)/shard_map/dot_general | solution.py:461
  72.4 1.7 %fusion = bf16[1,2048,256]{2,1,0:T(8,128)(2,1)} fusion(bf16[512,2048]{1,0:T(8,128)(2,1)S(1)} %bitcast.211, bf16[512,256]{1,0:T(8,128)(2,1)S(1)} %get-tuple-element.63), kind=kOutput, calls=%fused_computation.4 | convolution fusion | flops 537395200 | bytes 3407872 | tf_op jit(solution)/shard_map/dot_general | solution.py:461
  74.1 0.7 fusion.24
  74.9 0.5 copy-done.4
  75.3 2.1 %add_convert_fusion = bf16[512,2048]{1,0:T(8,128)(2,1)} fusion(f32[512,2048]{1,0:T(8,128)S(1)} %fusion.24, bf16[512,256]{1,0:T(8,128)(2,1)S(1)} %get-tuple-element.62, bf16[1,2048,256]{2,1,0:T(8,128)(2,1)S(1)} %copy-done.4), kind=kOutput, calls=%fused_computation | convolution fusion | flops 538968064 | bytes 7602176 | tf_op jit(solution)/shard_map/dot_general | solution.py:461
  77.4 41.3 %give_back.1 = (bf16[128,2048]{1,0:T(8,128)(2,1)}, bf16[8,128,512]{2,1,0:T(8,128)(2,1)}) custom-call(bf16[8,64,2048]{2,1,0:T(8,128)(2,1)} %bitcast.194, bf16[128,512]{1,0:T(8,128)(2,1)} %fusion.38.comb, bf16[128,512]{1,0:T(8,128)(2,1)} %copy-done.5, bf16[128,512]{1,0:T(8,128)(2,1)} %bitcast.201), custom_call_target="tpu_custom_call" | custom-call | tf_op jit(solution)/shard_map/give_back/pallas_call | solution.py:349
  118.8 2.9 %fusion.93 = f32[128,512]{0,1:T(8,128)} fusion(bf16[128,2048]{1,0:T(8,128)(2,1)} %get-tuple-element.19.resid, bf16[2048,512]{1,0:T(8,128)(2,1)S(1)} %copy-done), kind=kOutput, calls=%fused_computation.166 | convolution fusion | flops 268435456 | bytes 2883584 | tf_op jit(solution)/shard_map/dot_general | solution.py:582
  121.7 1.1 copy.218
  122.7 0.9 fusion.28
  123.6 0.8 fusion.29
  124.4 0.4 fusion.94
  124.8 1.0 fusion.18
  125.9 0.2 fusion.73
  126.0 0.2 fusion.61
  126.3 0.8 convolution_convert_fusion.4.state
  127.1 0.2 convolution_bitcast_fusion.2
  127.6 1.0 fusion.16
  128.6 0.7 copy.238
  129.3 31.3 %swap.1 = (bf16[8,128,256]{2,1,0:T(8,128)(2,1)}, bf16[8,2,128,256]{3,2,1,0:T(8,128)(2,1)}) custom-call(bf16[128,2048]{1,0:T(8,128)(2,1)} %get-tuple-element.19.resid, bf16[2,128,256]{2,1,0:T(8,128)(2,1)} %convolution_convert_fusion.4.state), custom_call_target="tpu_custom_call" | custom-call | tf_op jit(solution)/shard_map/swap/pallas_call | solution.py:412
  160.6 2.7 %convolution_bitcast_fusion = f32[256,512]{1,0:T(8,128)} fusion(bf16[8,128,256]{2,1,0:T(8,128)(2,1)} %get-tuple-element.20, bf16[8,128,512]{2,1,0:T(8,128)(2,1)} %get-tuple-element.21), kind=kOutput, calls=%fused_computation.12 | convolution fusion | flops 268435456 | bytes 2097152 | tf_op jit(solution)/shard_map/dot_general | solution.py:461
  163.3 0.3 multiply_reduce_fusion
  163.7 0.2 fusion.6
  163.9 0.2 fusion.49
  164.1 0.3 fusion.17
  164.4 0.7 copy.239
  165.1 0.8 copy.240
  (75 shorter events, 1.6 us)
Async XLA Ops:
  0.6 118.2 %copy-start = (bf16[2048,512]{1,0:T(8,128)(2,1)S(1)}, bf16[2048,512]{1,0:T(8,128)(2,1)}, u32[]{:S(2)}) copy-start(bf16[2048,512]{1,0:T(8,128)(2,1)} %param.20) | copy-start | bytes 6291460
  0.6 11.8 %copy-start.1 = (bf16[128,2,256]{2,1,0:T(2,128)(2,1)S(1)}, bf16[128,2,256]{2,1,0:T(2,128)(2,1)}, u32[]{:S(2)}) copy-start(bf16[128,2,256]{2,1,0:T(2,128)(2,1)} %param.18) | copy-start | bytes 393220
  0.8 57.7 %copy-start.21 = (pred[8]{0:T(512)(128)(4,1)}, pred[8]{0:T(512)(128)(4,1)S(1)}, u32[]{:S(2)}) copy-start(pred[8]{0:T(512)(128)(4,1)S(1)} %get-tuple-element.81) | copy-start | bytes 28
  1.6 13.2 %copy-start.12 = (pred[128]{0:T(512)(128)(4,1)}, pred[128]{0:T(512)(128)(4,1)S(1)}, u32[]{:S(2)}) copy-start(pred[128]{0:T(512)(128)(4,1)S(1)} %get-tuple-element.79) | copy-start | bytes 388
  1.6 13.2 %copy-start.14 = (pred[128]{0:T(512)(128)(4,1)}, pred[128]{0:T(512)(128)(4,1)S(1)}, u32[]{:S(2)}) copy-start(pred[128]{0:T(512)(128)(4,1)S(1)} %get-tuple-element.80) | copy-start | bytes 388
  1.6 13.2 %copy-start.16 = (s32[128]{0:T(128)}, s32[128]{0:T(128)S(1)}, u32[]{:S(2)}) copy-start(s32[128]{0:T(128)S(1)} %get-tuple-element.83) | copy-start | bytes 1540
  1.7 13.1 %copy-start.18 = (s32[128]{0:T(128)}, s32[128]{0:T(128)S(1)}, u32[]{:S(2)}) copy-start(s32[128]{0:T(128)S(1)} %get-tuple-element.84) | copy-start | bytes 1540
  7.1 9.7 %copy-start.6 = (f32[128,2]{0,1:T(2,128)}, f32[128,2]{0,1:T(2,128)S(1)}, u32[]{:S(2)}) copy-start(f32[128,2]{0,1:T(2,128)S(1)} %copy.201) | copy-start | bytes 3076
  8.0 60.9 %copy-start.8 = (f32[2,128]{1,0:T(2,128)}, f32[2,128]{1,0:T(2,128)S(1)}, u32[]{:S(2)}) copy-start(f32[2,128]{1,0:T(2,128)S(1)} %get-tuple-element.73) | copy-start | bytes 3076
  9.3 60.5 %copy-start.11 = (f32[128,2]{0,1:T(2,128)}, f32[128,2]{0,1:T(2,128)S(1)}, u32[]{:S(2)}) copy-start(f32[128,2]{0,1:T(2,128)S(1)} %copy.212) | copy-start | bytes 3076
  11.3 46.1 %copy-start.5 = (bf16[128,512]{1,0:T(8,128)(2,1)}, bf16[128,512]{1,0:T(8,128)(2,1)S(1)}, u32[]{:S(2)}) copy-start(bf16[128,512]{1,0:T(8,128)(2,1)S(1)} %constant_dynamic-slice_fusion.og) | copy-start | bytes 393220
  60.9 3.3 %copy-start.3 = (bf16[1,2048,256]{2,1,0:T(8,128)(2,1)S(1)}, bf16[1,2048,256]{2,1,0:T(8,128)(2,1)}, u32[]{:S(2)}) copy-start(bf16[1,2048,256]{2,1,0:T(8,128)(2,1)} %param.21) | copy-start | bytes 3145732
  60.9 3.3 %copy-start.23 = (bf16[8,64,2048]{2,1,0:T(8,128)(2,1)S(1)}, bf16[8,64,2048]{2,1,0:T(8,128)(2,1)}, u32[]{:S(2)}) copy-start(bf16[8,64,2048]{2,1,0:T(8,128)(2,1)} %get-tuple-element.15) | copy-start | bytes 6291460
  64.2 1.6 copy-start.24
  64.2 1.8 %copy-start.25 = (bf16[1,256,2048]{2,1,0:T(8,128)(2,1)S(1)}, bf16[1,256,2048]{2,1,0:T(8,128)(2,1)}, u32[]{:S(2)}) copy-start(bf16[1,256,2048]{2,1,0:T(8,128)(2,1)} %param.23) | copy-start | bytes 3145732
  74.1 1.2 copy-start.4
  122.7 3.5 %copy-start.9 = (f32[2,128]{1,0:T(2,128)S(1)}, f32[2,128]{1,0:T(2,128)}, u32[]{:S(2)}) copy-start(f32[2,128]{1,0:T(2,128)} %copy-done.8) | copy-start | bytes 3076
  127.3 35.9 %copy-start.7 = (f32[8,2]{1,0:T(8,128)S(1)}, f32[8,2]{1,0:T(8,128)}, u32[]{:S(2)}) copy-start(f32[8,2]{1,0:T(8,128)} %copy.231) | copy-start | bytes 196
  127.4 35.9 %copy-start.22 = (pred[8]{0:T(512)(128)(4,1)S(1)}, pred[8]{0:T(512)(128)(4,1)}, u32[]{:S(2)}) copy-start(pred[8]{0:T(512)(128)(4,1)} %copy-done.21) | copy-start | bytes 28
  128.5 35.1 %copy-start.10 = (f32[128,2]{0,1:T(2,128)S(1)}, f32[128,2]{0,1:T(2,128)}, u32[]{:S(2)}) copy-start(f32[128,2]{0,1:T(2,128)} %copy.230) | copy-start | bytes 3076
  160.5 2.8 %copy-start.2 = (bf16[8,2,128,256]{3,2,1,0:T(8,128)(2,1)S(1)}, bf16[8,2,128,256]{3,2,1,0:T(8,128)(2,1)}, u32[]{:S(2)}) copy-start(bf16[8,2,128,256]{3,2,1,0:T(8,128)(2,1)} %get-tuple-element.22) | copy-start | bytes 3145732
  160.5 3.6 %copy-start.13 = (pred[128]{0:T(512)(128)(4,1)S(1)}, pred[128]{0:T(512)(128)(4,1)}, u32[]{:S(2)}) copy-start(pred[128]{0:T(512)(128)(4,1)} %copy-done.12) | copy-start | bytes 388
  160.5 3.6 %copy-start.15 = (pred[128]{0:T(512)(128)(4,1)S(1)}, pred[128]{0:T(512)(128)(4,1)}, u32[]{:S(2)}) copy-start(pred[128]{0:T(512)(128)(4,1)} %copy-done.14) | copy-start | bytes 388
  160.6 3.6 %copy-start.17 = (s32[128]{0:T(128)S(1)}, s32[128]{0:T(128)}, u32[]{:S(2)}) copy-start(s32[128]{0:T(128)} %copy-done.16) | copy-start | bytes 1540
  160.6 3.6 %copy-start.19 = (s32[128]{0:T(128)S(1)}, s32[128]{0:T(128)}, u32[]{:S(2)}) copy-start(s32[128]{0:T(128)} %copy-done.18) | copy-start | bytes 1540
  160.6 3.6 %copy-start.20 = (f32[2,128]{1,0:T(2,128)S(1)}, f32[2,128]{1,0:T(2,128)}, u32[]{:S(2)}) copy-start(f32[2,128]{1,0:T(2,128)} %get-tuple-element.61) | copy-start | bytes 3076
